TPU v7x, 32 devices: a whole 2x2x4 slice. The times are simulated.
32 devices in a mesh: grp: 2 (over y), fs: 4 (over z), tp: 4 (over x, core).
Axes of the slice: x: 2, y: 2, z: 4, core: 2. Of those that a mesh axis runs over, the one named last changes fastest.
Arguments:
- tokens: bfloat16 [2048, 2048], P(('grp', 'fs'), 'tp'), parts along dimension 0, may hold values from -6 to 6
- recurrent_norm_gain: float32 [2048], replicated, may hold values from 0.1 to 1.9
- feedforward_norm_gain: float32 [2048], replicated, may hold values from 0.1 to 1.9
- gate_projection_weight: bfloat16 [2048, 2048], P('fs', 'tp'), may hold values from -0.125 to 0.125
- recurrent_projection_weight: bfloat16 [2048, 2048], P('fs', 'tp'), may hold values from -0.125 to 0.125
- convolution_kernel: bfloat16 [4, 2048], P(None, 'tp'), may hold values from -3 to 3
- decay_gate_matrix: bfloat16 [16, 128, 128], P('tp'), may hold values from -0.5 to 0.5
- input_gate_matrix: bfloat16 [16, 128, 128], P('tp'), may hold values from -0.5 to 0.5
- base_decay_logit: float32 [2048], P('tp'), may hold values from 3 to 9
- extra_log_decay: float32 [2048], P(('grp', 'fs')), parts along dimension 0, may hold values from -0.7 to 0
- output_projection_weight: bfloat16 [2048, 2048], P('tp', 'fs'), may hold values from -0.125 to 0.125
- up_projection_weight: bfloat16 [2048, 8192], P('fs', 'tp'), may hold values from -0.125 to 0.125
- down_projection_weight: bfloat16 [8192, 2048], P('tp', 'fs'), may hold values from -0.0625 to 0.0625
Outputs:
- layer_out: bfloat16 [2048, 2048], P(('grp', 'fs'), 'tp'), parts along dimension 0
There are 2 independent parts, one for each index of `grp`. A program takes and returns all parts, laid end to end along the dimension named above; an argument that names none is the same for every part. Nothing has to cross between parts.
All inputs are finite; a program needn't handle non-finite values.
Results may differ from a plain program's by a relative error of at most 0.018.
Values may be sent and summed in bfloat16 or wider, within the bound.
A program may use at most 64 MiB of HBM per device.

v0:
```python
import jax
import jax.numpy as jnp
from jax import lax
from jax.sharding import PartitionSpec as P


def rms_rows(values_in, norm_gain):
    values = values_in.astype(jnp.float32)
    inverse = lax.rsqrt(jnp.mean(values * values, axis=-1, keepdims=True) + 1e-06)
    return (values * inverse * norm_gain).astype(jnp.bfloat16)


def combine(earlier, later):
    return (earlier[0] * later[0], later[0] * earlier[1] + later[1])


def recurrent_state(
    recurrent_branch_rows,
    gate_branch_rows,
    convolution_kernel,
    decay_gate_matrix,
    input_gate_matrix,
    base_decay_logit,
    extra_log_decay,
):
    length = recurrent_branch_rows.shape[0]
    taps = convolution_kernel.shape[0]
    padded = jnp.pad(recurrent_branch_rows.astype(jnp.float32), ((taps - 1, 0), (0, 0)))
    conv_sum = jnp.zeros((length, recurrent_branch_rows.shape[1]), jnp.float32)
    for tap_index in range(taps):
        conv_sum = conv_sum + padded[tap_index : tap_index + length] * convolution_kernel[
            tap_index
        ].astype(jnp.float32)
    conv_rows = conv_sum.astype(jnp.bfloat16)
    blocks = decay_gate_matrix.shape[0]
    blocked = conv_rows.reshape(length, blocks, -1)
    recurrence_gate = jax.nn.sigmoid(
        jnp.einsum(
            "tni,nij->tnj", blocked, decay_gate_matrix, preferred_element_type=jnp.float32
        ).reshape(length, -1)
    )
    input_rate = jax.nn.sigmoid(
        jnp.einsum(
            "tni,nij->tnj", blocked, input_gate_matrix, preferred_element_type=jnp.float32
        ).reshape(length, -1)
    )
    decay_log_values = (
        -8.0 * jax.nn.softplus(-base_decay_logit) * recurrence_gate + extra_log_decay[:, None]
    )
    decay = jnp.exp(decay_log_values)
    drive = (
        jnp.sqrt(-jnp.expm1(2.0 * decay_log_values)) * input_rate * conv_rows.astype(jnp.float32)
    )
    _, hidden = lax.associative_scan(combine, (decay, drive), axis=0)
    return (hidden * gate_branch_rows.astype(jnp.float32)).astype(jnp.bfloat16)


def per_device(
    tokens,
    recurrent_norm_gain,
    feedforward_norm_gain,
    gate_projection_weight,
    recurrent_projection_weight,
    convolution_kernel,
    decay_gate_matrix,
    input_gate_matrix,
    base_decay_logit,
    extra_log_decay,
    output_projection_weight,
    up_projection_weight,
    down_projection_weight,
):
    whole_rows = lax.all_gather(tokens, "tp", axis=1, tiled=True)
    normed = rms_rows(whole_rows, recurrent_norm_gain)
    columns = normed
    gate_pre = jnp.dot(
        columns,
        lax.all_gather(gate_projection_weight, "fs", axis=0, tiled=True),
        preferred_element_type=jnp.float32,
    )
    recur_pre = jnp.dot(
        columns,
        lax.all_gather(recurrent_projection_weight, "fs", axis=0, tiled=True),
        preferred_element_type=jnp.float32,
    )
    gate_branch_rows = jax.nn.gelu(gate_pre).astype(jnp.bfloat16)
    recurrent_branch_rows = recur_pre.astype(jnp.bfloat16)
    mixed_output = recurrent_state(
        recurrent_branch_rows,
        gate_branch_rows,
        convolution_kernel,
        decay_gate_matrix,
        input_gate_matrix,
        base_decay_logit,
        extra_log_decay,
    )
    partials = jnp.dot(
        mixed_output,
        lax.all_gather(output_projection_weight, "fs", axis=1, tiled=True),
        preferred_element_type=jnp.float32,
    )
    residual = (
        tokens.astype(jnp.float32)
        + lax.psum_scatter(
            partials.astype(jnp.bfloat16), "tp", scatter_dimension=1, tiled=True
        ).astype(jnp.float32)
    ).astype(jnp.bfloat16)
    middle = lax.all_gather(residual, "tp", axis=1, tiled=True)
    channel_in = rms_rows(middle, feedforward_norm_gain)
    columns = channel_in
    upward = jnp.dot(
        columns,
        lax.all_gather(up_projection_weight, "fs", axis=0, tiled=True),
        preferred_element_type=jnp.float32,
    )
    positive = jnp.maximum(upward, 0.0)
    squared = (positive * positive).astype(jnp.bfloat16)
    down_terms = jnp.dot(
        squared,
        lax.all_gather(down_projection_weight, "fs", axis=1, tiled=True),
        preferred_element_type=jnp.float32,
    )
    summed_down = lax.psum_scatter(
        down_terms.astype(jnp.bfloat16), "tp", scatter_dimension=1, tiled=True
    ).astype(jnp.float32)
    return (residual.astype(jnp.float32) + summed_down).astype(jnp.bfloat16)


def solution(mesh):
    placed = (
        P(("grp", "fs"), "tp"),
        P(),
        P(),
        P("fs", "tp"),
        P("fs", "tp"),
        P(None, "tp"),
        P("tp", None, None),
        P("tp", None, None),
        P("tp"),
        P(("grp", "fs")),
        P("tp", "fs"),
        P("fs", "tp"),
        P("tp", "fs"),
    )
    return jax.shard_map(
        per_device, mesh=mesh, in_specs=placed, out_specs=P(("grp", "fs"), "tp"), check_vma=False
    )
```

profile of v0, /device:TPU:0, one launch (start us, length us, event | category | flops | bytes accessed | tf_op | source)
XLA Modules:
  0.0 558.3 jit_solution(17213416898491841167)
XLA Ops:
  6.5 0.7 all-gather.8.cloned.1.call-update
  7.3 0.0 all-gather.10.cloned.1.call-start
  7.3 0.7 all-gather.10.cloned.1.call-update
  8.0 0.0 all-gather.12.cloned.1.call-start
  8.1 0.7 all-gather.12.cloned.1.call-update
  8.7 0.0 all-gather.14.cloned.1.call-start
  8.8 0.5 all-gather.14.cloned.1.call-update
  9.3 0.0 reduce-scatter.3.cloned.1.call-start
  9.4 0.8 slice_convert_fusion.3
  10.2 0.7 fusion.55
  10.9 17.4 %all-gather.8.cloned.1.call-done = bf16[256,2048]{1,0:T(8,128)(2,1)} async-done(((bf16[256,512]{1,0:T(8,128)(2,1)}), bf16[256,2048]{1,0:T(8,128)(2,1)}) %all-gather.8.cloned.1.call-update) | async-done | bytes 1048592 | tf_op jit(solution)/shard_map/all_gather | solution.py:73
  28.4 1.5 fusion.2
  29.9 45.7 %all-gather.10.cloned.1.call-done = bf16[2048,512]{1,0:T(8,128)(2,1)} async-done(((bf16[512,512]{1,0:T(8,128)(2,1)}), bf16[2048,512]{1,0:T(8,128)(2,1)}) %all-gather.10.cloned.1.call-update) | async-done | bytes 2097168 | tf_op jit(solution)/shard_map/all_gather | solution.py:83
  75.6 2.7 fusion.14
  78.3 0.0 copy-start.5
  78.3 0.2 fusion.77
  78.6 0.0 copy-done
  78.6 0.3 fusion.11
  78.9 0.0 copy-start.4
  78.9 0.2 copy.22
  79.1 0.1 copy-done.5
  79.2 0.3 fusion.13
  79.5 0.2 copy.23
  79.8 0.7 fusion.29
  80.4 0.3 slice.215
  80.8 0.3 slice.216
  81.1 0.3 slice.214
  81.4 0.3 slice.218
  81.7 0.1 fusion.62
  81.8 0.1 slice.221
  82.0 0.1 slice.222
  82.1 0.1 slice.220
  82.2 0.1 slice.224
  83.1 0.2 slice.219
  83.3 0.2 slice.268
  83.5 0.3 slice.270
  83.9 0.3 slice.213
  84.9 0.1 pad.69
  85.0 0.1 fusion.41
  85.1 0.1 pad.68
  85.2 0.0 copy-start.2
  85.2 36.4 %all-gather.12.cloned.1.call-done = bf16[2048,512]{1,0:T(8,128)(2,1)} async-done(((bf16[512,512]{1,0:T(8,128)(2,1)}), bf16[2048,512]{1,0:T(8,128)(2,1)}) %all-gather.12.cloned.1.call-update) | async-done | bytes 2097168 | tf_op jit(solution)/shard_map/all_gather | solution.py:78
  121.7 45.9 %all-gather.14.cloned.1.call-done = bf16[512,2048]{1,0:T(8,128)(2,1)} async-done(((bf16[512,512]{1,0:T(8,128)(2,1)}), bf16[512,2048]{1,0:T(8,128)(2,1)}) %all-gather.14.cloned.1.call-update) | async-done | bytes 2097168 | tf_op jit(solution)/shard_map/all_gather | solution.py:99
  167.6 4.8 convolution_convert_fusion
  172.4 0.0 reduce-scatter.3.cloned.1.call-update
  172.4 0.0 all-gather.16.cloned.1.call-start
  172.5 23.7 %reduce-scatter.3.cloned.1.call-done = bf16[256,512]{1,0:T(8,128)(2,1)} async-done(((bf16[256,2048]{1,0:T(8,128)(2,1)}), bf16[256,512]{1,0:T(8,128)(2,1)}) %reduce-scatter.3.cloned.1.call-update) | async-done | bytes 262160 | tf_op jit(solution)/shard_map/reduce_scatter | solution.py:104
  196.1 1.7 add_convert_fusion.1
  197.9 0.0 all-gather.16.cloned.1.call-update
  197.9 0.0 all-gather.18.cloned.1.call-start
  197.9 0.7 all-gather.18.cloned.1.call-update
  198.6 0.0 copy-start.7
  198.6 0.0 all-gather.20.cloned.1.call-start
  198.7 0.7 all-gather.20.cloned.1.call-update
  199.4 0.0 reduce-scatter.5.cloned.1.call-start
  199.4 15.3 %all-gather.16.cloned.1.call-done = bf16[256,2048]{1,0:T(8,128)(2,1)} async-done(((bf16[256,512]{1,0:T(8,128)(2,1)}), bf16[256,2048]{1,0:T(8,128)(2,1)}) %all-gather.16.cloned.1.call-update) | async-done | bytes 1048592 | tf_op jit(solution)/shard_map/all_gather | solution.py:108
  214.7 1.5 fusion.5
  216.3 0.0 copy-start.1
  216.3 149.7 %all-gather.18.cloned.1.call-done = bf16[2048,2048]{1,0:T(8,128)(2,1)} async-done(((bf16[512,2048]{1,0:T(8,128)(2,1)}), bf16[2048,2048]{1,0:T(8,128)(2,1)}) %all-gather.18.cloned.1.call-update) | async-done | bytes 8388624 | tf_op jit(solution)/shard_map/all_gather | solution.py:113
  366.0 149.4 %all-gather.20.cloned.1.call-done = bf16[2048,2048]{1,0:T(8,128)(2,1)} async-done(((bf16[2048,512]{1,0:T(8,128)(2,1)}), bf16[2048,2048]{1,0:T(8,128)(2,1)}) %all-gather.20.cloned.1.call-update) | async-done | bytes 8388624 | tf_op jit(solution)/shard_map/all_gather | solution.py:120
  515.4 11.6 %convolution_convert_fusion.1 = bf16[256,2048]{1,0:T(8,128)(2,1)} fusion(bf16[2048,2048]{1,0:T(8,128)(2,1)} %all-gather.20.cloned.1.call-done, bf16[2048,2048]{1,0:T(8,128)(2,1)} %all-gather.18.cloned.1.call-done, bf16[256,2048]{1,0:T(8,128)(2,1)} %all-gather.16.cloned.1.call-done, f32[2048]{0:T(1024)S(1)} %copy-done.7, f32[256]{0:T(256)S(1)} %add_rsqrt_fusion), kind=kOutput, calls=%fused_computation.8 | convolution fusion | flops 4299161600 | bytes 18883584 | tf_op jit(solution)/shard_map/dot_general | solution.py:118
  527.0 0.0 reduce-scatter.5.cloned.1.call-update
  527.0 23.1 %reduce-scatter.5.cloned.1.call-done = bf16[256,512]{1,0:T(8,128)(2,1)} async-done(((bf16[256,2048]{1,0:T(8,128)(2,1)}), bf16[256,512]{1,0:T(8,128)(2,1)}) %reduce-scatter.5.cloned.1.call-update) | async-done | bytes 262160 | tf_op jit(solution)/shard_map/reduce_scatter | solution.py:123
  550.1 1.7 add_convert_fusion
  (85 shorter events, 1.3 us)
Async XLA Ops:
  6.5 72.0 %copy-start = (bf16[4,128,128]{2,1,0:T(8,128)(2,1)S(1)}, bf16[4,128,128]{2,1,0:T(8,128)(2,1)}, u32[]{:S(2)}) copy-start(bf16[4,128,128]{2,1,0:T(8,128)(2,1)} %param.19) | copy-start | bytes 393220
  6.5 69.1 %copy-start.6 = (f32[2048]{0:T(1024)S(1)}, f32[2048]{0:T(1024)}, u32[]{:S(2)}) copy-start(f32[2048]{0:T(1024)} %param.14) | copy-start | bytes 24580
  6.5 21.8 %all-gather.8.cloned.1.call-start = ((), (), s32[]{:S(2)}) async-start(), calls=%async_computation.2 | async-start | bytes 1310720 | tf_op jit(solution)/shard_map/all_gather | solution.py:73
  7.3 68.3 %all-gather.10.cloned.1.call-start = ((), (), s32[]{:S(2)}) async-start(), calls=%async_computation.3 | async-start | bytes 2621440 | tf_op jit(solution)/shard_map/all_gather | solution.py:83
  8.0 113.7 %all-gather.12.cloned.1.call-start = ((), (), s32[]{:S(2)}) async-start(), calls=%async_computation.4 | async-start | bytes 2621440 | tf_op jit(solution)/shard_map/all_gather | solution.py:78
  8.7 158.9 %all-gather.14.cloned.1.call-start = ((), (), s32[]{:S(2)}) async-start(), calls=%async_computation.5 | async-start | bytes 2621440 | tf_op jit(solution)/shard_map/all_gather | solution.py:99
  9.3 186.8 %reduce-scatter.3.cloned.1.call-start = ((), (), s32[]{:S(2)}) async-start(), calls=%async_computation.6 | async-start | bytes 1310720 | tf_op jit(solution)/shard_map/reduce_scatter | solution.py:104
  78.3 0.9 copy-start.5
  78.9 0.8 copy-start.4
  84.9 82.7 %copy-start.3 = (bf16[256,2048]{1,0:T(8,128)(2,1)S(1)}, bf16[256,2048]{1,0:T(8,128)(2,1)}, u32[]{:S(2)}) copy-start(bf16[256,2048]{1,0:T(8,128)(2,1)} %all-gather.8.cloned.1.call-done) | copy-start | bytes 3145732
  85.2 110.9 %copy-start.2 = (bf16[256,512]{1,0:T(8,128)(2,1)S(1)}, bf16[256,512]{1,0:T(8,128)(2,1)}, u32[]{:S(2)}) copy-start(bf16[256,512]{1,0:T(8,128)(2,1)} %param.13) | copy-start | bytes 786436
  172.4 42.3 %all-gather.16.cloned.1.call-start = ((), (), s32[]{:S(2)}) async-start(), calls=%async_computation.7 | async-start | bytes 1310720 | tf_op jit(solution)/shard_map/all_gather | solution.py:108
  197.9 168.1 %all-gather.18.cloned.1.call-start = ((), (), s32[]{:S(2)}) async-start(), calls=%async_computation.8 | async-start | bytes 10485760 | tf_op jit(solution)/shard_map/all_gather | solution.py:113
  198.6 316.7 %copy-start.7 = (f32[2048]{0:T(1024)S(1)}, f32[2048]{0:T(1024)}, u32[]{:S(2)}) copy-start(f32[2048]{0:T(1024)} %param.15) | copy-start | bytes 24580
  198.6 316.7 %all-gather.20.cloned.1.call-start = ((), (), s32[]{:S(2)}) async-start(), calls=%async_computation.9 | async-start | bytes 10485760 | tf_op jit(solution)/shard_map/all_gather | solution.py:120
  199.4 350.7 %reduce-scatter.5.cloned.1.call-start = ((), (), s32[]{:S(2)}) async-start(), calls=%async_computation.10 | async-start | bytes 1310720 | tf_op jit(solution)/shard_map/reduce_scatter | solution.py:123
  216.3 333.8 %copy-start.1 = (bf16[256,512]{1,0:T(8,128)(2,1)S(1)}, bf16[256,512]{1,0:T(8,128)(2,1)}, u32[]{:S(2)}) copy-start(bf16[256,512]{1,0:T(8,128)(2,1)} %add_convert_fusion.1) | copy-start | bytes 786436
Sparse Core Ops, SparseCore 0:
  8.9 19.4 all-gather.7
  29.9 45.6 all-gather.9
  77.2 44.4 all-gather.11
  123.1 44.4 all-gather.13
  172.5 23.5 reduce-scatter.2
  198.0 16.6 all-gather.15
  216.3 149.6 all-gather.17
  367.5 147.7 all-gather.19
  527.1 22.9 reduce-scatter.4
where the time goes:
time: 559 us; the launch traced here: 558 us
  waiting for transfers between devices  511 us (91%)
  matrix products  19.7 us (4%)
  between operations  13.8 us (2%)
  other arithmetic  9.49 us (2%)
    all_gather x1, waiting for transfers between devices, per_device(): lax.all_gather(up_projection_weight, 'fs', axis=0, tiled=True)  150 us
    all_gather x1, waiting for transfers between devices, per_device(): lax.all_gather(down_projection_weight, 'fs', axis=1, tiled=True)  149 us
    all_gather x1, waiting for transfers between devices, per_device(): lax.all_gather(output_projection_weight, 'fs', axis=1, tiled=True)  45.9 us
    all_gather x1, waiting for transfers between devices, per_device(): lax.all_gather(recurrent_projection_weight, 'fs', axis=0, tiled=True)  45.7 us
    all_gather x1, waiting for transfers between devices, per_device(): lax.all_gather(gate_projection_weight, 'fs', axis=0, tiled=True)  36.4 us
    reduce_scatter x1, waiting for transfers between devices, per_device(): lax.psum_scatter(partials.astype(jnp.bfloat16), 'tp', scatter_dimension=1...  23.7 us
    reduce_scatter x1, waiting for transfers between devices, per_device(): lax.psum_scatter(down_terms.astype(jnp.bfloat16), 'tp', scatter_dimension...  23.1 us
    all_gather x1, waiting for transfers between devices, per_device(): whole_rows = lax.all_gather(tokens, 'tp', axis=1, tiled=True)  17.4 us
  transfers between devices with their start and end apart: 9, of which 9 were waited for; matrix products, arithmetic and copies ran while one was open for 2% of the time, Pallas kernels for 0%

commit v1 on v0

--- a/solution.py
+++ b/solution.py
@@ -126,6 +126,109 @@
     return (residual.astype(jnp.float32) + summed_down).astype(jnp.bfloat16)
 
 
+def exchange_blocks(weight, split_axis, join_axis):
+    count, mine = lax.axis_size("fs"), lax.axis_index("fs")
+    planes, plane = lax.axis_size("grp"), lax.axis_index("grp")
+    width = weight.shape[split_axis] // count
+    depth = weight.shape[join_axis]
+
+    def piece(owner):
+        return lax.dynamic_slice_in_dim(weight, owner * width, width, split_axis)
+
+    shape = list(weight.shape)
+    shape[split_axis] = width
+    shape[join_axis] = depth * count
+    joined = jnp.zeros(shape, weight.dtype)
+
+    def put(joined, value, row, column):
+        place = [0, 0]
+        place[join_axis] += column
+        place[0] = place[0] + row
+        return lax.dynamic_update_slice(joined, value, place)
+
+    joined = put(joined, piece(mine), 0, mine * depth)
+    share = (depth if join_axis == 0 else width) // planes
+    for step in range(1, count):
+        target = lax.rem(mine + step, count)
+        source = lax.rem(mine - step + count, count)
+        part = lax.dynamic_slice_in_dim(piece(target), plane * share, share, 0)
+        part = lax.ppermute(part, "fs", [(i, (i + step) % count) for i in range(count)])
+        joined = put(joined, part, plane * share, source * depth)
+        for turn in range(1, planes):
+            other = lax.ppermute(part, "grp", [(i, (i + turn) % planes) for i in range(planes)])
+            origin = lax.rem(plane - turn + planes, planes)
+            joined = put(joined, other, origin * share, source * depth)
+    return joined
+
+
+def gather_all(rows):
+    rows = lax.all_gather(rows, "fs", axis=0, tiled=True)
+    return lax.all_gather(rows, "tp", axis=1, tiled=True)
+
+
+def scatter_sum(partials):
+    partials = lax.psum_scatter(partials, "tp", scatter_dimension=1, tiled=True)
+    return lax.psum_scatter(partials, "fs", scatter_dimension=0, tiled=True)
+
+
+def per_device_owned(
+    tokens,
+    recurrent_norm_gain,
+    feedforward_norm_gain,
+    gate_projection_weight,
+    recurrent_projection_weight,
+    convolution_kernel,
+    decay_gate_matrix,
+    input_gate_matrix,
+    base_decay_logit,
+    extra_log_decay,
+    output_projection_weight,
+    up_projection_weight,
+    down_projection_weight,
+):
+    count, mine = lax.axis_size("fs"), lax.axis_index("fs")
+    length = tokens.shape[0]
+
+    def own(value, axis):
+        width = value.shape[axis] // count
+        return lax.dynamic_slice_in_dim(value, mine * width, width, axis)
+
+    gate_weight = exchange_blocks(gate_projection_weight, 1, 0)
+    recur_weight = exchange_blocks(recurrent_projection_weight, 1, 0)
+    out_weight = exchange_blocks(output_projection_weight, 0, 1)
+    up_weight = exchange_blocks(up_projection_weight, 1, 0)
+    down_weight = exchange_blocks(down_projection_weight, 0, 1)
+    extra = lax.all_gather(extra_log_decay, "fs", axis=0, tiled=True)
+
+    normed = rms_rows(gather_all(tokens), recurrent_norm_gain)
+    gate_rows = jax.nn.gelu(
+        jnp.dot(normed, gate_weight, preferred_element_type=jnp.float32)
+    ).astype(jnp.bfloat16)
+    recur_rows = jnp.dot(normed, recur_weight, preferred_element_type=jnp.float32).astype(
+        jnp.bfloat16
+    )
+    mixed = jax.vmap(recurrent_state, in_axes=(0, 0, None, None, None, None, 0))(
+        recur_rows.reshape(count, length, -1),
+        gate_rows.reshape(count, length, -1),
+        own(convolution_kernel, 1),
+        own(decay_gate_matrix, 0),
+        own(input_gate_matrix, 0),
+        own(base_decay_logit, 0),
+        extra.reshape(count, length),
+    ).reshape(count * length, -1)
+    partials = jnp.dot(mixed, out_weight, preferred_element_type=jnp.float32)
+    summed = scatter_sum(partials.astype(jnp.bfloat16))
+    residual = (tokens.astype(jnp.float32) + summed.astype(jnp.float32)).astype(jnp.bfloat16)
+    channel_in = rms_rows(gather_all(residual), feedforward_norm_gain)
+    positive = jnp.maximum(
+        jnp.dot(channel_in, up_weight, preferred_element_type=jnp.float32), 0.0
+    )
+    squared = (positive * positive).astype(jnp.bfloat16)
+    down_terms = jnp.dot(squared, down_weight, preferred_element_type=jnp.float32)
+    summed_down = scatter_sum(down_terms.astype(jnp.bfloat16)).astype(jnp.float32)
+    return (residual.astype(jnp.float32) + summed_down).astype(jnp.bfloat16)
+
+
 def solution(mesh):
     placed = (
         P(("grp", "fs"), "tp"),
@@ -142,6 +245,13 @@
         P("fs", "tp"),
         P("tp", "fs"),
     )
-    return jax.shard_map(
-        per_device, mesh=mesh, in_specs=placed, out_specs=P(("grp", "fs"), "tp"), check_vma=False
-    )
+    owners = mesh.shape["fs"] * mesh.shape["tp"]
+
+    def run(*arrays):
+        owned = arrays[6].shape[0] % owners == 0
+        body = per_device_owned if owned else per_device
+        return jax.shard_map(
+            body, mesh=mesh, in_specs=placed, out_specs=P(("grp", "fs"), "tp"), check_vma=False
+        )(*arrays)
+
+    return run

time: 559 us -> 571 us (1.021)
  waiting for transfers between devices: 511 us -> 241 us
  local copies, waits for them, and re-layouts: 4.25 us -> 220 us
  starting transfers between devices: 0.31 us -> 38.3 us
  other arithmetic: 9.49 us -> 23.7 us
  blocking collectives: 0 us -> 11 us
    all_gather x7 -> x4, waiting for transfers between devices: 460 us -> 59 us  [the longest x2 58.9 us: gather_all(): rows = lax.all_gather(rows, 'fs', axis=0, tiled=True)]
    slice x46 -> x43, local copies, waits for them, and re-layouts: 3.39 us -> 122 us  [recurrent_state(): _, hidden = lax.associative_scan(combine, (decay, drive), axis=0)]
    reduce_scatter x2 -> x4, waiting for transfers between devices: 46.8 us -> 150 us  [the longest x2 91.3 us: scatter_sum(): partials = lax.psum_scatter(partials, 'tp', scatter_dimension=1, tiled=True)]
    dynamic_update_slice x0 -> x34, local copies, waits for them, and re-layouts: none -> 42.7 us  [put(): return lax.dynamic_update_slice(joined, value, place)]
    ppermute x0 -> x30, starting transfers between devices: none -> 38.1 us  [the longest x15 21.6 us: exchange_blocks(): lax.ppermute(part, 'fs', [(i, (i + step) % count) for i in range(count)])]
    pad x14, local copies, waits for them, and re-layouts: 0.35 us -> 38 us  [recurrent_state(): _, hidden = lax.associative_scan(combine, (decay, drive), axis=0)]
    ppermute x0 -> x30, waiting for transfers between devices: none -> 31.1 us  [the longest x15 30.5 us: exchange_blocks(): lax.ppermute(part, 'fs', [(i, (i + step) % count) for i in range(count)])]
    all_gather x0 -> x1, blocking collectives: none -> 11 us  [per_device_owned(): extra = lax.all_gather(extra_log_decay, 'fs', axis=0, tiled=True)]
  transfers between devices with their start and end apart: 9 -> 38, of which waited for: 9 -> 11; matrix products, arithmetic and copies ran while one was open for 2% -> 9% of each run, Pallas kernels for 0% -> 0%
where the time goes in v1:
time: 571 us; the launch traced here: 567 us
  waiting for transfers between devices  241 us (42%)
  local copies, waits for them, and re-layouts  220 us (39%)
  starting transfers between devices  38.3 us (7%)
  other arithmetic  23.7 us (4%)
  matrix products  18 us (3%)
  between operations  14.8 us (3%)
  blocking collectives  11 us (2%)
    slice x43, local copies, waits for them, and re-layouts, recurrent_state(): _, hidden = lax.associative_scan(combine, (decay, drive), axis=0)  122 us
    reduce_scatter x2, waiting for transfers between devices, scatter_sum(): partials = lax.psum_scatter(partials, 'tp', scatter_dimension=1, tiled=True)  91.3 us
    reduce_scatter x2, waiting for transfers between devices, scatter_sum(): return lax.psum_scatter(partials, 'fs', scatter_dimension=0, tiled=True)  59 us
    all_gather x2, waiting for transfers between devices, gather_all(): rows = lax.all_gather(rows, 'fs', axis=0, tiled=True)  58.9 us
    dynamic_update_slice x34, local copies, waits for them, and re-layouts, put(): return lax.dynamic_update_slice(joined, value, place)  42.7 us
    pad x14, local copies, waits for them, and re-layouts, recurrent_state(): _, hidden = lax.associative_scan(combine, (decay, drive), axis=0)  38 us
    ppermute x15, waiting for transfers between devices, exchange_blocks(): lax.ppermute(part, 'fs', [(i, (i + step) % count) for i in range(count)])  30.5 us
    ppermute x15, starting transfers between devices, exchange_blocks(): lax.ppermute(part, 'fs', [(i, (i + step) % count) for i in range(count)])  21.6 us
  transfers between devices with their start and end apart: 38, of which 11 were waited for; matrix products, arithmetic and copies ran while one was open for 9% of the time, Pallas kernels for 0%

profile of v1, /device:TPU:0, one launch (start us, length us, event | category | flops | bytes accessed | tf_op | source)
XLA Modules:
  0.0 566.7 jit_solution(12668084185289499219)
XLA Ops:
  7.3 32.3 %all-gather.6.cloned.1.call-done = bf16[1024,512]{1,0:T(8,128)(2,1)} async-done(((bf16[256,512]{1,0:T(8,128)(2,1)}), bf16[1024,512]{1,0:T(8,128)(2,1)}) %all-gather.6.cloned.1.call-update) | async-done | bytes 1048592 | tf_op jit(solution)/shard_map/all_gather | solution.py:165
  40.8 1.8 collective-permute-start.16
  42.9 1.8 collective-permute-start.14
  45.9 2.1 collective-permute-start.10
  48.4 11.0 %all-gather = f32[4,1,256]{2,1,0:T(1,128)S(1)} all-gather(f32[1,1,256]{2,1,0:T(1,128)S(1)} %bitcast.75), channel_id=1, replica_groups=mesh['grp'=2,'fs'=4,'tp'=4] {'fs'}, dimensions={0}, use_global_device_ids=true | all-gather | bytes 5120 | tf_op jit(solution)/shard_map/all_gather | solution.py:201
  60.9 1.6 dynamic-slice_dynamic-update-slice_fusion.3
  69.7 1.8 collective-permute-done
  71.5 4.9 collective-permute-start.4
  78.5 1.7 dynamic_update_slice.122
  81.3 1.7 dynamic_update_slice.124
  93.2 3.2 fusion
  100.4 8.7 %slice.270 = f32[4,127,128]{1,2,0:T(8,128)S(1)} slice(f32[4,256,128]{1,2,0:T(8,128)S(1)} %fusion.23), slice={[0:4:1], [2:256:2], [0:128:1]} | slice | bytes 520192 | tf_op jit(solution)/shard_map/vmap()/slice | solution.py:54
  109.1 9.0 %slice.216 = f32[4,128,128]{1,2,0:T(8,128)S(1)} slice(f32[4,256,128]{1,2,0:T(8,128)S(1)} %fusion.23), slice={[0:4:1], [1:256:2], [0:128:1]} | slice | bytes 524288 | tf_op jit(solution)/shard_map/vmap()/slice | solution.py:54
  118.1 8.8 %slice.215 = f32[4,128,128]{1,2,0:T(8,128)S(1)} slice(f32[4,256,128]{1,2,0:T(8,128)S(1)} %fusion.23), slice={[0:4:1], [0:255:2], [0:128:1]} | slice | bytes 524288 | tf_op jit(solution)/shard_map/vmap()/slice | solution.py:54
  126.9 8.8 %slice.218 = f32[4,128,128]{1,2,0:T(8,128)S(1)} slice(f32[4,256,128]{1,2,0:T(8,128)S(1)} %get-tuple-element.40), slice={[0:4:1], [0:255:2], [0:128:1]} | slice | bytes 524288 | tf_op jit(solution)/shard_map/vmap()/slice | solution.py:54
  135.7 9.0 %slice.214 = f32[4,128,128]{1,2,0:T(8,128)S(1)} slice(f32[4,256,128]{1,2,0:T(8,128)S(1)} %get-tuple-element.40), slice={[0:4:1], [1:256:2], [0:128:1]} | slice | bytes 524288 | tf_op jit(solution)/shard_map/vmap()/slice | solution.py:54
  144.7 9.3 %slice.213 = f32[4,127,128]{1,2,0:T(8,128)} slice(f32[4,256,128]{1,2,0:T(8,128)S(1)} %get-tuple-element.40), slice={[0:4:1], [2:256:2], [0:128:1]} | slice | bytes 520192 | tf_op jit(solution)/shard_map/vmap()/slice | solution.py:54
  154.2 4.5 slice.224
  158.6 4.5 slice.220
  163.2 4.9 slice.219
  168.1 5.1 slice.268
  173.2 4.5 slice.222
  177.7 4.5 slice.221
  182.3 2.3 slice.230
  184.6 2.4 slice.226
  187.0 2.9 slice.225
  189.9 2.9 slice.266
  192.8 2.4 slice.228
  195.2 2.5 slice.227
  200.3 1.9 slice.231
  202.2 1.8 slice.264
  228.5 3.2 fusion.42
  238.4 1.7 add_multiply_fusion.5
  251.3 2.4 pad.64
  253.6 2.7 pad.65
  257.6 4.5 pad.66
  262.1 4.6 pad.67
  267.0 8.9 %pad.68 = f32[4,256,128]{1,2,0:T(8,128)S(1)} pad(f32[4,128,128]{1,2,0:T(8,128)S(1)} %pad_maximum_fusion.3, f32[]{:T(128)} %constant.208.clone.1), padding=0_0_0x0_1_1x0_0_0 | pad | bytes 786436 | tf_op jit(solution)/shard_map/vmap()/pad | solution.py:54
  275.8 8.9 %pad.69 = f32[4,256,128]{1,2,0:T(8,128)S(1)} pad(f32[4,128,128]{1,2,0:T(8,128)S(1)} %add.483, f32[]{:T(128)} %constant.208.clone.1), padding=0_0_0x1_0_1x0_0_0 | pad | bytes 786436 | tf_op jit(solution)/shard_map/vmap()/pad | solution.py:54
  285.0 3.2 convolution_convert_fusion.1
  288.3 44.4 %reduce-scatter.5.cloned.1.call-done = bf16[1024,512]{1,0:T(8,128)(2,1)} async-done(((bf16[1024,2048]{1,0:T(8,128)(2,1)}), bf16[1024,512]{1,0:T(8,128)(2,1)}) %reduce-scatter.5.cloned.1.call-update) | async-done | bytes 1048592 | tf_op jit(solution)/shard_map/reduce_scatter | solution.py:170
  332.7 29.4 %reduce-scatter.7.cloned.1.call-done = bf16[256,512]{1,0:T(8,128)(2,1)} async-done(((bf16[1024,512]{1,0:T(8,128)(2,1)}), bf16[256,512]{1,0:T(8,128)(2,1)}) %reduce-scatter.7.cloned.1.call-update) | async-done | bytes 262160 | tf_op jit(solution)/shard_map/reduce_scatter | solution.py:171
  362.1 1.7 add_convert_fusion.1
  363.9 26.6 %all-gather.10.cloned.1.call-done = bf16[1024,512]{1,0:T(8,128)(2,1)} async-done(((bf16[256,512]{1,0:T(8,128)(2,1)}), bf16[1024,512]{1,0:T(8,128)(2,1)}) %all-gather.10.cloned.1.call-update) | async-done | bytes 1048592 | tf_op jit(solution)/shard_map/all_gather | solution.py:165
  390.6 2.4 fusion.65
  393.1 1.8 collective-permute-start.22
  395.1 1.8 collective-permute-start.20
  397.1 2.1 collective-permute-start.28
  399.6 9.8 %collective-permute-done.22 = bf16[256,512]{1,0:T(8,128)(2,1)S(1)} collective-permute-done((bf16[256,512]{1,0:T(8,128)(2,1)}, bf16[256,512]{1,0:T(8,128)(2,1)S(1)}, u32[]{:S(2)}, u32[]{:S(2)}) %collective-permute-start.22) | collective-permute-done | bytes 262176 | tf_op jit(solution)/shard_map/ppermute | solution.py:155
  409.4 3.9 collective-permute-start.26
  414.8 1.6 broadcast_in_dim.8
  418.4 13.1 %collective-permute-done.20 = bf16[256,512]{1,0:T(8,128)(2,1)} collective-permute-done((bf16[256,512]{1,0:T(8,128)(2,1)}, bf16[256,512]{1,0:T(8,128)(2,1)}, u32[]{:S(2)}, u32[]{:S(2)}) %collective-permute-start.20) | collective-permute-done | bytes 262176 | tf_op jit(solution)/shard_map/ppermute | solution.py:155
  435.0 5.8 %collective-permute-done.26 = bf16[256,512]{1,0:T(8,128)(2,1)} collective-permute-done((bf16[256,512]{1,0:T(8,128)(2,1)S(1)}, bf16[256,512]{1,0:T(8,128)(2,1)}, u32[]{:S(2)}, u32[]{:S(2)}) %collective-permute-start.26) | collective-permute-done | bytes 262176 | tf_op jit(solution)/shard_map/ppermute | solution.py:155
  443.3 4.3 dynamic_update_slice.134
  449.9 3.1 dynamic_update_slice.135
  452.9 4.7 dynamic_update_slice.136
  457.6 3.5 dynamic_update_slice.137
  461.2 4.7 dynamic_update_slice.138
  465.8 3.5 dynamic_update_slice.139
  469.5 3.1 fusion.3
  472.6 8.6 %convolution_convert_fusion = bf16[1024,2048]{1,0:T(8,128)(2,1)} fusion(bf16[512,2048]{1,0:T(8,128)(2,1)} %dynamic_update_slice.139, bf16[2048,512]{1,0:T(8,128)(2,1)S(1)} %constant_dynamic-update-slice_fusion, bf16[1024,2048]{1,0:T(8,128)(2,1)} %all-gather.12.cloned.1.call-done, f32[2048]{0:T(1024)S(1)} %copy-done.13, f32[1024]{0:T(1024)S(1)} %add_rsqrt_fusion), kind=kOutput, calls=%fused_computation.13 | convolution fusion | flops 4307025920 | bytes 12595200 | tf_op jit(solution)/shard_map/dot_general | solution.py:227
  481.3 47.0 %reduce-scatter.9.cloned.1.call-done = bf16[1024,512]{1,0:T(8,128)(2,1)} async-done(((bf16[1024,2048]{1,0:T(8,128)(2,1)}), bf16[1024,512]{1,0:T(8,128)(2,1)}) %reduce-scatter.9.cloned.1.call-update) | async-done | bytes 1048592 | tf_op jit(solution)/shard_map/reduce_scatter | solution.py:170
  528.3 29.6 %reduce-scatter.11.cloned.1.call-done = bf16[256,512]{1,0:T(8,128)(2,1)} async-done(((bf16[1024,512]{1,0:T(8,128)(2,1)}), bf16[256,512]{1,0:T(8,128)(2,1)}) %reduce-scatter.11.cloned.1.call-update) | async-done | bytes 262160 | tf_op jit(solution)/shard_map/reduce_scatter | solution.py:171
  557.8 1.7 add_convert_fusion
  (215 shorter events, 89.3 us)
Async XLA Ops:
  6.5 92.1 %copy-start = (bf16[4,128,128]{2,1,0:T(8,128)(2,1)S(1)}, bf16[4,128,128]{2,1,0:T(8,128)(2,1)}, u32[]{:S(2)}) copy-start(bf16[4,128,128]{2,1,0:T(8,128)(2,1)} %param.19) | copy-start | bytes 393220
  6.5 41.8 %copy-start.11 = (f32[256]{0:T(256)S(1)}, f32[256]{0:T(256)}, u32[]{:S(2)}) copy-start(f32[256]{0:T(256)} %param.22) | copy-start | bytes 3076
  6.5 33.1 %all-gather.6.cloned.1.call-start = ((), (), s32[]{:S(2)}) async-start(), calls=%async_computation.4 | async-start | bytes 1310720 | tf_op jit(solution)/shard_map/all_gather | solution.py:165
  7.3 85.9 %all-gather.8.cloned.1.call-start = ((), (), s32[]{:S(2)}) async-start(), calls=%async_computation.5 | async-start | bytes 5242880 | tf_op jit(solution)/shard_map/all_gather | solution.py:166
  39.6 23.9 %copy-start.10 = (bf16[512,512]{1,0:T(8,128)(2,1)S(1)}, bf16[512,512]{1,0:T(8,128)(2,1)}, u32[]{:S(2)}) copy-start(bf16[512,512]{1,0:T(8,128)(2,1)} %param.17) | copy-start | bytes 1572868
  39.7 293.0 %reduce-scatter.5.cloned.1.call-start = ((), (), s32[]{:S(2)}) async-start(), calls=%async_computation.6 | async-start | bytes 5242880 | tf_op jit(solution)/shard_map/reduce_scatter | solution.py:170
  40.8 25.0 %collective-permute-start.16 = (bf16[64,512]{1,0:T(8,128)(2,1)S(1)}, bf16[64,512]{1,0:T(8,128)(2,1)S(1)}, u32[]{:S(2)}, u32[]{:S(2)}) collective-permute-start(bf16[64,512]{1,0:T(8,128)(2,1)S(1)} %get-tuple-element.11), channel_id=1, source_target_pairs={{0,12},{4,0},{8,4},{12,8},{1,13},{5,1},{9,5},{13,9},{2,14},{6,2},{... | collective-permute-start | bytes 196616 | tf_op jit(solution)/shard_map/ppermute | solution.py:155
  42.7 21.9 %collective-permute-start.12 = (bf16[64,512]{1,0:T(8,128)(2,1)S(1)}, bf16[64,512]{1,0:T(8,128)(2,1)S(1)}, u32[]{:S(2)}, u32[]{:S(2)}) collective-permute-start(bf16[64,512]{1,0:T(8,128)(2,1)S(1)} %get-tuple-element.12), channel_id=1, source_target_pairs={{0,4},{4,8},{8,12},{12,0},{1,5},{5,9},{9,13},{13,1},{2,6},{6,10},{... | collective-permute-start | bytes 196616 | tf_op jit(solution)/shard_map/ppermute | solution.py:155
  42.9 24.1 %collective-permute-start.14 = (bf16[64,512]{1,0:T(8,128)(2,1)S(1)}, bf16[64,512]{1,0:T(8,128)(2,1)S(1)}, u32[]{:S(2)}, u32[]{:S(2)}) collective-permute-start(bf16[64,512]{1,0:T(8,128)(2,1)S(1)} %get-tuple-element.13), channel_id=1, source_target_pairs={{0,8},{4,12},{8,0},{12,4},{1,9},{5,13},{9,1},{13,5},{2,10},{6,14},... | collective-permute-start | bytes 196616 | tf_op jit(solution)/shard_map/ppermute | solution.py:155
  45.9 38.2 %collective-permute-start.10 = (bf16[256,128]{1,0:T(8,128)(2,1)S(1)}, bf16[256,128]{1,0:T(8,128)(2,1)S(1)}, u32[]{:S(2)}, u32[]{:S(2)}) collective-permute-start(bf16[256,128]{1,0:T(8,128)(2,1)S(1)} %get-tuple-element.17), channel_id=1, source_target_pairs={{0,12},{4,0},{8,4},{12,8},{1,13},{5,1},{9,5},{13,9},{2,14},{6,2},{... | collective-permute-start | bytes 196616 | tf_op jit(solution)/shard_map/ppermute | solution.py:155
  48.0 19.9 %collective-permute-start.6 = (bf16[256,128]{1,0:T(8,128)(2,1)S(1)}, bf16[256,128]{1,0:T(8,128)(2,1)S(1)}, u32[]{:S(2)}, u32[]{:S(2)}) collective-permute-start(bf16[256,128]{1,0:T(8,128)(2,1)S(1)} %get-tuple-element.18), channel_id=1, source_target_pairs={{0,4},{4,8},{8,12},{12,0},{1,5},{5,9},{9,13},{13,1},{2,6},{6,10},{... | collective-permute-start | bytes 196616 | tf_op jit(solution)/shard_map/ppermute | solution.py:155
  64.6 6.9 %collective-permute-start = (bf16[256,128]{1,0:T(8,128)(2,1)S(1)}, bf16[256,128]{1,0:T(8,128)(2,1)S(1)}, u32[]{:S(2)}, u32[]{:S(2)}) collective-permute-start(bf16[256,128]{1,0:T(8,128)(2,1)S(1)} %get-tuple-element.15), channel_id=1, source_target_pairs={{0,4},{4,8},{8,12},{12,0},{1,5},{5,9},{9,13},{13,1},{2,6},{6,10},{... | collective-permute-start | bytes 196616 | tf_op jit(solution)/shard_map/ppermute | solution.py:155
  65.8 10.6 %collective-permute-start.13 = (bf16[64,512]{1,0:T(8,128)(2,1)S(1)}, bf16[64,512]{1,0:T(8,128)(2,1)S(1)}, u32[]{:S(2)}, u32[]{:S(2)}) collective-permute-start(bf16[64,512]{1,0:T(8,128)(2,1)S(1)} %collective-permute-done.12), channel_id=1, source_target_pairs={{0,16},{16,0},{1,17},{17,1},{2,18},{18,2},{3,19},{19,3},{4,20},{20... | collective-permute-start | bytes 196616 | tf_op jit(solution)/shard_map/ppermute | solution.py:158
  67.0 4.4 collective-permute-start.17
  67.9 8.5 %collective-permute-start.15 = (bf16[64,512]{1,0:T(8,128)(2,1)S(1)}, bf16[64,512]{1,0:T(8,128)(2,1)S(1)}, u32[]{:S(2)}, u32[]{:S(2)}) collective-permute-start(bf16[64,512]{1,0:T(8,128)(2,1)S(1)} %collective-permute-done.14), channel_id=1, source_target_pairs={{0,16},{16,0},{1,17},{17,1},{2,18},{18,2},{3,19},{19,3},{4,20},{20... | collective-permute-start | bytes 196616 | tf_op jit(solution)/shard_map/ppermute | solution.py:158
  71.5 13.8 %collective-permute-start.8 = (bf16[256,128]{1,0:T(8,128)(2,1)S(1)}, bf16[256,128]{1,0:T(8,128)(2,1)S(1)}, u32[]{:S(2)}, u32[]{:S(2)}) collective-permute-start(bf16[256,128]{1,0:T(8,128)(2,1)S(1)} %get-tuple-element.19), channel_id=1, source_target_pairs={{0,8},{4,12},{8,0},{12,4},{1,9},{5,13},{9,1},{13,5},{2,10},{6,14},... | collective-permute-start | bytes 196616 | tf_op jit(solution)/shard_map/ppermute | solution.py:155
  71.5 14.7 %collective-permute-start.4 = (bf16[256,128]{1,0:T(8,128)(2,1)S(1)}, bf16[256,128]{1,0:T(8,128)(2,1)S(1)}, u32[]{:S(2)}, u32[]{:S(2)}) collective-permute-start(bf16[256,128]{1,0:T(8,128)(2,1)S(1)} %get-tuple-element.14), channel_id=1, source_target_pairs={{0,12},{4,0},{8,4},{12,8},{1,13},{5,1},{9,5},{13,9},{2,14},{6,2},{... | collective-permute-start | bytes 196616 | tf_op jit(solution)/shard_map/ppermute | solution.py:155
  76.3 11.0 %collective-permute-start.2 = (bf16[256,128]{1,0:T(8,128)(2,1)S(1)}, bf16[256,128]{1,0:T(8,128)(2,1)S(1)}, u32[]{:S(2)}, u32[]{:S(2)}) collective-permute-start(bf16[256,128]{1,0:T(8,128)(2,1)S(1)} %get-tuple-element.16), channel_id=1, source_target_pairs={{0,8},{4,12},{8,0},{12,4},{1,9},{5,13},{9,1},{13,5},{2,10},{6,14},... | collective-permute-start | bytes 196616 | tf_op jit(solution)/shard_map/ppermute | solution.py:155
  76.3 11.9 %collective-permute-start.7 = (bf16[256,128]{1,0:T(8,128)(2,1)S(1)}, bf16[256,128]{1,0:T(8,128)(2,1)S(1)}, u32[]{:S(2)}, u32[]{:S(2)}) collective-permute-start(bf16[256,128]{1,0:T(8,128)(2,1)S(1)} %collective-permute-done.6), channel_id=1, source_target_pairs={{0,16},{16,0},{1,17},{17,1},{2,18},{18,2},{3,19},{19,3},{4,20},{20... | collective-permute-start | bytes 196616 | tf_op jit(solution)/shard_map/ppermute | solution.py:158
  84.1 6.5 %collective-permute-start.1 = (bf16[256,128]{1,0:T(8,128)(2,1)S(1)}, bf16[256,128]{1,0:T(8,128)(2,1)S(1)}, u32[]{:S(2)}, u32[]{:S(2)}) collective-permute-start(bf16[256,128]{1,0:T(8,128)(2,1)S(1)} %collective-permute-done), channel_id=1, source_target_pairs={{0,16},{16,0},{1,17},{17,1},{2,18},{18,2},{3,19},{19,3},{4,20},{20... | collective-permute-start | bytes 196616 | tf_op jit(solution)/shard_map/ppermute | solution.py:158
  85.3 7.2 %collective-permute-start.11 = (bf16[256,128]{1,0:T(8,128)(2,1)S(1)}, bf16[256,128]{1,0:T(8,128)(2,1)S(1)}, u32[]{:S(2)}, u32[]{:S(2)}) collective-permute-start(bf16[256,128]{1,0:T(8,128)(2,1)S(1)} %collective-permute-done.10), channel_id=1, source_target_pairs={{0,16},{16,0},{1,17},{17,1},{2,18},{18,2},{3,19},{19,3},{4,20},{20... | collective-permute-start | bytes 196616 | tf_op jit(solution)/shard_map/ppermute | solution.py:158
  86.2 4.5 collective-permute-start.9
  87.3 5.2 collective-permute-start.5
  88.2 4.3 collective-permute-start.3
  93.2 3.2 copy-start.12
  93.2 3.5 copy-start.2
  100.4 53.8 %copy-start.5 = (f32[4,256,128]{1,2,0:T(8,128)}, f32[4,256,128]{1,2,0:T(8,128)S(1)}, u32[]{:S(2)}) copy-start(f32[4,256,128]{1,2,0:T(8,128)S(1)} %fusion.23) | copy-start | bytes 1572868
  225.1 3.4 copy-start.3
  238.4 4.1 copy-start.8
  256.3 10.4 %copy-start.7 = (f32[4,127,128]{1,2,0:T(8,128)S(1)}, f32[4,127,128]{1,2,0:T(8,128)}, u32[]{:S(2)}) copy-start(f32[4,127,128]{1,2,0:T(8,128)} %slice.213) | copy-start | bytes 780292
  257.4 9.4 %slice-start = ((f32[4,256,128]{1,2,0:T(8,128)}), f32[4,1,128]{1,2,0:T(8,128)S(1)}, s32[]{:S(2)}) async-start(f32[4,256,128]{1,2,0:T(8,128)} %copy-done.5), calls=%async_computation.12 | async-start | bytes 524288 | tf_op jit(solution)/shard_map/vmap()/slice | solution.py:54
  288.2 73.9 %copy-start.6 = (bf16[256,512]{1,0:T(8,128)(2,1)S(1)}, bf16[256,512]{1,0:T(8,128)(2,1)}, u32[]{:S(2)}) copy-start(bf16[256,512]{1,0:T(8,128)(2,1)} %param.13) | copy-start | bytes 786436
  288.2 73.9 %reduce-scatter.7.cloned.1.call-start = ((), (), s32[]{:S(2)}) async-start(), calls=%async_computation.7 | async-start | bytes 1310720 | tf_op jit(solution)/shard_map/reduce_scatter | solution.py:171
  332.7 64.2 %copy-start.9 = (bf16[2048,512]{1,0:T(8,128)(2,1)S(1)}, bf16[2048,512]{1,0:T(8,128)(2,1)}, u32[]{:S(2)}) copy-start(bf16[2048,512]{1,0:T(8,128)(2,1)} %param.25) | copy-start | bytes 6291460
  332.7 57.8 %all-gather.10.cloned.1.call-start = ((), (), s32[]{:S(2)}) async-start(), calls=%async_computation.8 | async-start | bytes 1310720 | tf_op jit(solution)/shard_map/all_gather | solution.py:165
  363.9 105.6 %all-gather.12.cloned.1.call-start = ((), (), s32[]{:S(2)}) async-start(), calls=%async_computation.9 | async-start | bytes 5242880 | tf_op jit(solution)/shard_map/all_gather | solution.py:166
  390.6 137.7 %reduce-scatter.9.cloned.1.call-start = ((), (), s32[]{:S(2)}) async-start(), calls=%async_computation.10 | async-start | bytes 5242880 | tf_op jit(solution)/shard_map/reduce_scatter | solution.py:170
  393.1 16.3 %collective-permute-start.22 = (bf16[256,512]{1,0:T(8,128)(2,1)}, bf16[256,512]{1,0:T(8,128)(2,1)S(1)}, u32[]{:S(2)}, u32[]{:S(2)}) collective-permute-start(bf16[256,512]{1,0:T(8,128)(2,1)} %get-tuple-element.5), channel_id=1, source_target_pairs={{0,12},{4,0},{8,4},{12,8},{1,13},{5,1},{9,5},{13,9},{2,14},{6,2},{... | collective-permute-start | bytes 786440 | tf_op jit(solution)/shard_map/ppermute | solution.py:155
  394.9 18.4 %collective-permute-start.18 = (bf16[256,512]{1,0:T(8,128)(2,1)S(1)}, bf16[256,512]{1,0:T(8,128)(2,1)}, u32[]{:S(2)}, u32[]{:S(2)}) collective-permute-start(bf16[256,512]{1,0:T(8,128)(2,1)S(1)} %get-tuple-element.6), channel_id=1, source_target_pairs={{0,4},{4,8},{8,12},{12,0},{1,5},{5,9},{9,13},{13,1},{2,6},{6,10},{... | collective-permute-start | bytes 786440 | tf_op jit(solution)/shard_map/ppermute | solution.py:155
  395.1 36.4 %collective-permute-start.20 = (bf16[256,512]{1,0:T(8,128)(2,1)}, bf16[256,512]{1,0:T(8,128)(2,1)}, u32[]{:S(2)}, u32[]{:S(2)}) collective-permute-start(bf16[256,512]{1,0:T(8,128)(2,1)} %get-tuple-element.7), channel_id=1, source_target_pairs={{0,8},{4,12},{8,0},{12,4},{1,9},{5,13},{9,1},{13,5},{2,10},{6,14},... | collective-permute-start | bytes 786440 | tf_op jit(solution)/shard_map/ppermute | solution.py:155
  397.1 35.9 %collective-permute-start.28 = (bf16[256,512]{1,0:T(8,128)(2,1)S(1)}, bf16[256,512]{1,0:T(8,128)(2,1)}, u32[]{:S(2)}, u32[]{:S(2)}) collective-permute-start(bf16[256,512]{1,0:T(8,128)(2,1)S(1)} %get-tuple-element.8), channel_id=1, source_target_pairs={{0,12},{4,0},{8,4},{12,8},{1,13},{5,1},{9,5},{13,9},{2,14},{6,2},{... | collective-permute-start | bytes 786440 | tf_op jit(solution)/shard_map/ppermute | solution.py:155
  399.1 34.4 %collective-permute-start.24 = (bf16[256,512]{1,0:T(8,128)(2,1)S(1)}, bf16[256,512]{1,0:T(8,128)(2,1)}, u32[]{:S(2)}, u32[]{:S(2)}) collective-permute-start(bf16[256,512]{1,0:T(8,128)(2,1)S(1)} %get-tuple-element.9), channel_id=1, source_target_pairs={{0,4},{4,8},{8,12},{12,0},{1,5},{5,9},{9,13},{13,1},{2,6},{6,10},{... | collective-permute-start | bytes 786440 | tf_op jit(solution)/shard_map/ppermute | solution.py:155
  409.4 31.4 %collective-permute-start.26 = (bf16[256,512]{1,0:T(8,128)(2,1)S(1)}, bf16[256,512]{1,0:T(8,128)(2,1)}, u32[]{:S(2)}, u32[]{:S(2)}) collective-permute-start(bf16[256,512]{1,0:T(8,128)(2,1)S(1)} %get-tuple-element.10), channel_id=1, source_target_pairs={{0,8},{4,12},{8,0},{12,4},{1,9},{5,13},{9,1},{13,5},{2,10},{6,14},... | collective-permute-start | bytes 786440 | tf_op jit(solution)/shard_map/ppermute | solution.py:155
  413.3 34.2 %collective-permute-start.19 = (bf16[256,512]{1,0:T(8,128)(2,1)}, bf16[256,512]{1,0:T(8,128)(2,1)}, u32[]{:S(2)}, u32[]{:S(2)}) collective-permute-start(bf16[256,512]{1,0:T(8,128)(2,1)} %collective-permute-done.18), channel_id=1, source_target_pairs={{0,16},{16,0},{1,17},{17,1},{2,18},{18,2},{3,19},{19,3},{4,20},{20... | collective-permute-start | bytes 786440 | tf_op jit(solution)/shard_map/ppermute | solution.py:158
  431.5 37.9 %collective-permute-start.21 = (bf16[256,512]{1,0:T(8,128)(2,1)}, bf16[256,512]{1,0:T(8,128)(2,1)S(1)}, u32[]{:S(2)}, u32[]{:S(2)}) collective-permute-start(bf16[256,512]{1,0:T(8,128)(2,1)} %collective-permute-done.20), channel_id=1, source_target_pairs={{0,16},{16,0},{1,17},{17,1},{2,18},{18,2},{3,19},{19,3},{4,20},{20... | collective-permute-start | bytes 786440 | tf_op jit(solution)/shard_map/ppermute | solution.py:158
  433.0 32.8 %collective-permute-start.29 = (bf16[256,512]{1,0:T(8,128)(2,1)}, bf16[256,512]{1,0:T(8,128)(2,1)S(1)}, u32[]{:S(2)}, u32[]{:S(2)}) collective-permute-start(bf16[256,512]{1,0:T(8,128)(2,1)} %collective-permute-done.28), channel_id=1, source_target_pairs={{0,16},{16,0},{1,17},{17,1},{2,18},{18,2},{3,19},{19,3},{4,20},{20... | collective-permute-start | bytes 786440 | tf_op jit(solution)/shard_map/ppermute | solution.py:158
  433.6 16.3 %collective-permute-start.25 = (bf16[256,512]{1,0:T(8,128)(2,1)}, bf16[256,512]{1,0:T(8,128)(2,1)S(1)}, u32[]{:S(2)}, u32[]{:S(2)}) collective-permute-start(bf16[256,512]{1,0:T(8,128)(2,1)} %collective-permute-done.24), channel_id=1, source_target_pairs={{0,16},{16,0},{1,17},{17,1},{2,18},{18,2},{3,19},{19,3},{4,20},{20... | collective-permute-start | bytes 786440 | tf_op jit(solution)/shard_map/ppermute | solution.py:158
  440.8 16.8 %collective-permute-start.27 = (bf16[256,512]{1,0:T(8,128)(2,1)}, bf16[256,512]{1,0:T(8,128)(2,1)S(1)}, u32[]{:S(2)}, u32[]{:S(2)}) collective-permute-start(bf16[256,512]{1,0:T(8,128)(2,1)} %collective-permute-done.26), channel_id=1, source_target_pairs={{0,16},{16,0},{1,17},{17,1},{2,18},{18,2},{3,19},{19,3},{4,20},{20... | collective-permute-start | bytes 786440 | tf_op jit(solution)/shard_map/ppermute | solution.py:158
  447.5 21.9 %collective-permute-start.23 = (bf16[256,512]{1,0:T(8,128)(2,1)S(1)}, bf16[256,512]{1,0:T(8,128)(2,1)S(1)}, u32[]{:S(2)}, u32[]{:S(2)}) collective-permute-start(bf16[256,512]{1,0:T(8,128)(2,1)S(1)} %collective-permute-done.22), channel_id=1, source_target_pairs={{0,16},{16,0},{1,17},{17,1},{2,18},{18,2},{3,19},{19,3},{4,20},{20... | collective-permute-start | bytes 786440 | tf_op jit(solution)/shard_map/ppermute | solution.py:158
  469.5 3.1 copy-start.13
  481.2 78.4 %copy-start.1 = (bf16[4,128,128]{2,1,0:T(8,128)(2,1)S(1)}, bf16[4,128,128]{2,1,0:T(8,128)(2,1)}, u32[]{:S(2)}) copy-start(bf16[4,128,128]{2,1,0:T(8,128)(2,1)} %param.19) | copy-start | bytes 393220
  481.2 76.7 %copy-start.4 = (bf16[256,512]{1,0:T(8,128)(2,1)S(1)}, bf16[256,512]{1,0:T(8,128)(2,1)}, u32[]{:S(2)}) copy-start(bf16[256,512]{1,0:T(8,128)(2,1)} %add_convert_fusion.1) | copy-start | bytes 786436
  481.2 76.6 %reduce-scatter.11.cloned.1.call-start = ((), (), s32[]{:S(2)}) async-start(), calls=%async_computation.11 | async-start | bytes 1310720 | tf_op jit(solution)/shard_map/reduce_scatter | solution.py:171
Sparse Core Ops, SparseCore 0:
  8.9 30.6 all-gather.5
  41.2 33.8 all-gather.7
  288.4 44.2 reduce-scatter.4
  334.8 27.2 reduce-scatter.6
  364.0 26.4 all-gather.9
  391.9 33.8 all-gather.11
  481.3 46.8 reduce-scatter.8
  530.5 27.2 reduce-scatter.10

commit v2 on v1

--- a/solution.py
+++ b/solution.py
@@ -1,7 +1,13 @@
+import functools
+
 import jax
 import jax.numpy as jnp
 from jax import lax
+from jax.experimental import pallas as pl
+from jax.experimental.pallas import tpu as pltpu
 from jax.sharding import PartitionSpec as P
+
+MESH = pl.DeviceIdType.MESH
 
 
 def rms_rows(values_in, norm_gain):
@@ -161,14 +167,263 @@
     return joined
 
 
-def gather_all(rows):
-    rows = lax.all_gather(rows, "fs", axis=0, tiled=True)
-    return lax.all_gather(rows, "tp", axis=1, tiled=True)
-
-
-def scatter_sum(partials):
-    partials = lax.psum_scatter(partials, "tp", scatter_dimension=1, tiled=True)
-    return lax.psum_scatter(partials, "fs", scatter_dimension=0, tiled=True)
+def steps_by_distance(count):
+    return sorted(range(1, count), key=lambda step: (min(step, count - step), step))
+
+
+def greet(count, place, row):
+    barrier = pltpu.get_barrier_semaphore()
+    peers = [{"fs": lax.rem(place + step, count)} for step in range(1, count)]
+    peers += [{"tp": row ^ 1}, {"tp": row ^ 2}]
+    for peer in peers:
+        pl.semaphore_signal(barrier, inc=1, device_id=peer, device_id_type=MESH)
+    pl.semaphore_wait(barrier, len(peers))
+
+
+def gather_kernel(count, own_ref, gain_ref, out_ref, held, send_z, send_x, send_c, arrived):
+    place, row = lax.axis_index("fs"), lax.axis_index("tp")
+    across, beside, corner = row ^ 2, row ^ 1, row ^ 3
+    length, width = own_ref.shape
+    greet(count, place, row)
+
+    def copy(source, at, send_sem, peer):
+        return pltpu.make_async_remote_copy(
+            src_ref=source,
+            dst_ref=held.at[at[0], at[1]],
+            send_sem=send_sem,
+            recv_sem=arrived.at[at[0], at[1]],
+            device_id=peer,
+            device_id_type=MESH,
+        )
+
+    started = []
+
+    def send(source, at, send_sem, peer):
+        moving = copy(source, at, send_sem, peer)
+        moving.start()
+        started.append(moving)
+
+    def wait(at):
+        copy(held.at[at[0], at[1]], at, arrived.at[at[0], at[1]], {"tp": beside}).wait_recv()
+
+    order = steps_by_distance(count)
+    for step in order:
+        send(own_ref, (place, row), send_z.at[step], {"fs": lax.rem(place + step, count)})
+    send(own_ref, (place, row), send_x.at[0], {"tp": across})
+    send(own_ref, (place, row), send_c.at[0, 0], {"tp": beside})
+    held[place, row] = own_ref[...]
+    for step in [0] + order:
+        origin = lax.rem(place - step + count, count)
+        if step:
+            wait((origin, row))
+            block = held.at[origin, row]
+            send(block, (origin, row), send_x.at[step], {"tp": across})
+            send(block, (origin, row), send_c.at[0, step], {"tp": beside})
+        wait((origin, across))
+        send(held.at[origin, across], (origin, across), send_c.at[1, step], {"tp": beside})
+    tile = 64
+    for step in [0] + order:
+        origin = lax.rem(place - step + count, count)
+        wait((origin, beside))
+        wait((origin, corner))
+
+        def normalise(index, carry):
+            rows = pl.ds(pl.multiple_of(index * tile, tile), tile)
+            parts = [held[origin, part, rows].astype(jnp.float32) for part in range(4)]
+            total = sum(jnp.sum(part * part, axis=-1, keepdims=True) for part in parts)
+            inverse = lax.rsqrt(total / (4 * width) + 1e-06)
+            at = pl.ds(pl.multiple_of(origin * length + index * tile, tile), tile)
+            for number, part in enumerate(parts):
+                columns = pl.ds(number * width, width)
+                out_ref[at, columns] = (part * inverse * gain_ref[:, columns]).astype(
+                    out_ref.dtype
+                )
+            return carry
+
+        lax.fori_loop(0, length // tile, normalise, 0)
+    for moving in started:
+        moving.wait_send()
+
+
+def gather_normed(rows, norm_gain, number):
+    count = lax.axis_size("fs")
+    length, width = rows.shape
+    vmem = pl.BlockSpec(memory_space=pltpu.VMEM)
+    dma = pltpu.SemaphoreType.DMA
+    return pl.pallas_call(
+        functools.partial(gather_kernel, count),
+        out_shape=jax.ShapeDtypeStruct((count * length, 4 * width), rows.dtype),
+        in_specs=[vmem, vmem],
+        out_specs=vmem,
+        scratch_shapes=[
+            pltpu.VMEM((count, 4, length, width), rows.dtype),
+            dma((count,)),
+            dma((count,)),
+            dma((2, count)),
+            dma((count, 4)),
+        ],
+        compiler_params=pltpu.CompilerParams(
+            collective_id=number, has_side_effects=True, vmem_limit_bytes=24 * 2**20
+        ),
+        cost_estimate=pl.CostEstimate(flops=10**9, bytes_accessed=10**8, transcendentals=0),
+    )(rows, norm_gain.reshape(1, -1))
+
+
+def scatter_kernel(
+    count, terms_ref, base_ref, out_ref,
+    from_core, to_x, from_x, to_z, from_z, send_c, recv_c, send_x, recv_x, send_z, recv_z,
+):
+    place, row = lax.axis_index("fs"), lax.axis_index("tp")
+    across, beside, corner = row ^ 2, row ^ 1, row ^ 3
+    length, width = base_ref.shape
+    greet(count, place, row)
+    started = []
+
+    def copy(source, target, send_sem, recv_sem, peer):
+        return pltpu.make_async_remote_copy(
+            src_ref=source,
+            dst_ref=target,
+            send_sem=send_sem,
+            recv_sem=recv_sem,
+            device_id=peer,
+            device_id_type=MESH,
+        )
+
+    def send(*given):
+        moving = copy(*given)
+        moving.start()
+        started.append(moving)
+
+    def block(step, part):
+        owner = lax.rem(place + step, count)
+        return (
+            pl.ds(pl.multiple_of(owner * length, length), length),
+            pl.ds(pl.multiple_of(part * width, width), width),
+        )
+
+    def core_copy(step, side):
+        part = corner if side else beside
+        return (
+            terms_ref.at[block(step, part)],
+            from_core.at[side, step],
+            send_c.at[side, step],
+            recv_c.at[side, step],
+            {"tp": beside},
+        )
+
+    def x_copy(step):
+        return (to_x.at[step], from_x.at[step], send_x.at[step], recv_x.at[step], {"tp": across})
+
+    def z_copy(step):
+        peer = {"fs": lax.rem(place + step, count)}
+        return (to_z.at[step], from_z.at[step], send_z.at[step], recv_z.at[step], peer)
+
+    order = steps_by_distance(count)[::-1] + [0]
+    for step in order:
+        for side in (1, 0):
+            send(*core_copy(step, side))
+    wide = jnp.float32
+    for step in order:
+        copy(*core_copy(step, 1)).wait_recv()
+        mine = terms_ref[block(step, across)].astype(wide)
+        to_x[step] = (mine + from_core[1, step].astype(wide)).astype(to_x.dtype)
+        send(*x_copy(step))
+    total = base_ref[...].astype(wide)
+    summed = None
+    for step in order:
+        copy(*core_copy(step, 0)).wait_recv()
+        copy(*x_copy(step)).wait_recv()
+        mine = terms_ref[block(step, row)].astype(wide) + from_core[0, step].astype(wide)
+        mine = mine + from_x[step].astype(wide)
+        if step:
+            to_z[step] = mine.astype(to_z.dtype)
+            send(*z_copy(step))
+        else:
+            summed = mine
+    for step in order[:-1]:
+        copy(*z_copy(step)).wait_recv()
+        summed = summed + from_z[step].astype(wide)
+    out_ref[...] = (total + summed).astype(out_ref.dtype)
+    for moving in started:
+        moving.wait_send()
+
+
+def scatter_added(terms, base, number):
+    count = lax.axis_size("fs")
+    vmem = pl.BlockSpec(memory_space=pltpu.VMEM)
+    dma = pltpu.SemaphoreType.DMA
+    blocks = pltpu.VMEM((count,) + base.shape, base.dtype)
+    return pl.pallas_call(
+        functools.partial(scatter_kernel, count),
+        out_shape=jax.ShapeDtypeStruct(base.shape, base.dtype),
+        in_specs=[vmem, vmem],
+        out_specs=vmem,
+        scratch_shapes=[pltpu.VMEM((2, count) + base.shape, base.dtype)]
+        + [blocks] * 4
+        + [dma((2, count))] * 2
+        + [dma((count,))] * 4,
+        compiler_params=pltpu.CompilerParams(
+            collective_id=number, has_side_effects=True, vmem_limit_bytes=24 * 2**20
+        ),
+        cost_estimate=pl.CostEstimate(flops=10**9, bytes_accessed=10**8, transcendentals=0),
+    )(terms, base)
+
+
+def recurrence_kernel(
+    gate_ref, recur_ref, taps_ref, decay_map_ref, input_map_ref, rate_ref, extra_ref, out_ref
+):
+    wide = jnp.float32
+    recur = recur_ref[...].astype(jnp.bfloat16).astype(wide)
+    length = recur.shape[0]
+    position = lax.broadcasted_iota(jnp.int32, recur.shape, 0)
+    taps = taps_ref.shape[0]
+    conv = recur * taps_ref[taps - 1 : taps].astype(wide)
+    for tap in range(taps - 1):
+        back = taps - 1 - tap
+        earlier = jnp.where(position >= back, pltpu.roll(recur, back, 0), 0.0)
+        conv = conv + earlier * taps_ref[tap : tap + 1].astype(wide)
+    conv_rows = conv.astype(jnp.bfloat16)
+    recur_gate = jax.nn.sigmoid(
+        jnp.dot(conv_rows, decay_map_ref[0], preferred_element_type=wide)
+    )
+    input_rate = jax.nn.sigmoid(
+        jnp.dot(conv_rows, input_map_ref[0], preferred_element_type=wide)
+    )
+    log_decay = rate_ref[...] * recur_gate + extra_ref[...]
+    decay = jnp.exp(log_decay)
+    spread = -jnp.tanh(log_decay) * (decay * decay + 1.0)
+    drive = jnp.sqrt(spread) * input_rate * conv_rows.astype(wide)
+    back = 1
+    while back < length:
+        inside = position >= back
+        drive = drive + decay * jnp.where(inside, pltpu.roll(drive, back, 0), 0.0)
+        if back * 2 < length:
+            decay = decay * jnp.where(inside, pltpu.roll(decay, back, 0), 1.0)
+        back *= 2
+    gate_rows = jax.nn.gelu(gate_ref[...]).astype(jnp.bfloat16)
+    out_ref[...] = (drive * gate_rows.astype(wide)).astype(out_ref.dtype)
+
+
+def recurrence(both, taps, decay_map, input_map, rate, extra, count):
+    blocks, size, _ = decay_map.shape
+    length = both.shape[0] // count
+    return pl.pallas_call(
+        recurrence_kernel,
+        grid=(count, blocks),
+        out_shape=jax.ShapeDtypeStruct((count * length, blocks * size), jnp.bfloat16),
+        in_specs=[
+            pl.BlockSpec((length, size), lambda s, n: (s, n)),
+            pl.BlockSpec((length, size), lambda s, n: (s, n + blocks)),
+            pl.BlockSpec((taps.shape[0], size), lambda s, n: (0, n)),
+            pl.BlockSpec((1, size, size), lambda s, n: (n, 0, 0)),
+            pl.BlockSpec((1, size, size), lambda s, n: (n, 0, 0)),
+            pl.BlockSpec((1, size), lambda s, n: (0, n)),
+            pl.BlockSpec((length, 1), lambda s, n: (s, 0)),
+        ],
+        out_specs=pl.BlockSpec((length, size), lambda s, n: (s, n)),
+        compiler_params=pltpu.CompilerParams(vmem_limit_bytes=24 * 2**20),
+        cost_estimate=pl.CostEstimate(flops=10**8, bytes_accessed=10**7, transcendentals=10**6),
+    )(both, both, taps, decay_map, input_map, rate.reshape(1, -1), extra.reshape(-1, 1))
 
 
 def per_device_owned(
@@ -187,46 +442,41 @@
     down_projection_weight,
 ):
     count, mine = lax.axis_size("fs"), lax.axis_index("fs")
-    length = tokens.shape[0]
 
     def own(value, axis):
         width = value.shape[axis] // count
         return lax.dynamic_slice_in_dim(value, mine * width, width, axis)
 
-    gate_weight = exchange_blocks(gate_projection_weight, 1, 0)
-    recur_weight = exchange_blocks(recurrent_projection_weight, 1, 0)
+    depth = gate_projection_weight.shape[0]
+    paired = [
+        weight.reshape(depth, count, -1)
+        for weight in (gate_projection_weight, recurrent_projection_weight)
+    ]
+    both_weight = exchange_blocks(jnp.concatenate(paired, axis=2).reshape(depth, -1), 1, 0)
     out_weight = exchange_blocks(output_projection_weight, 0, 1)
     up_weight = exchange_blocks(up_projection_weight, 1, 0)
     down_weight = exchange_blocks(down_projection_weight, 0, 1)
     extra = lax.all_gather(extra_log_decay, "fs", axis=0, tiled=True)
 
-    normed = rms_rows(gather_all(tokens), recurrent_norm_gain)
-    gate_rows = jax.nn.gelu(
-        jnp.dot(normed, gate_weight, preferred_element_type=jnp.float32)
-    ).astype(jnp.bfloat16)
-    recur_rows = jnp.dot(normed, recur_weight, preferred_element_type=jnp.float32).astype(
-        jnp.bfloat16
-    )
-    mixed = jax.vmap(recurrent_state, in_axes=(0, 0, None, None, None, None, 0))(
-        recur_rows.reshape(count, length, -1),
-        gate_rows.reshape(count, length, -1),
+    normed = gather_normed(tokens, recurrent_norm_gain, 1)
+    mixed = recurrence(
+        jnp.dot(normed, both_weight, preferred_element_type=jnp.float32),
         own(convolution_kernel, 1),
         own(decay_gate_matrix, 0),
         own(input_gate_matrix, 0),
-        own(base_decay_logit, 0),
-        extra.reshape(count, length),
-    ).reshape(count * length, -1)
+        -8.0 * jax.nn.softplus(-own(base_decay_logit, 0)),
+        extra,
+        count,
+    )
     partials = jnp.dot(mixed, out_weight, preferred_element_type=jnp.float32)
-    summed = scatter_sum(partials.astype(jnp.bfloat16))
-    residual = (tokens.astype(jnp.float32) + summed.astype(jnp.float32)).astype(jnp.bfloat16)
-    channel_in = rms_rows(gather_all(residual), feedforward_norm_gain)
+    residual = scatter_added(partials.astype(jnp.bfloat16), tokens, 2)
+    channel_in = gather_normed(residual, feedforward_norm_gain, 3)
     positive = jnp.maximum(
         jnp.dot(channel_in, up_weight, preferred_element_type=jnp.float32), 0.0
     )
     squared = (positive * positive).astype(jnp.bfloat16)
     down_terms = jnp.dot(squared, down_weight, preferred_element_type=jnp.float32)
-    summed_down = scatter_sum(down_terms.astype(jnp.bfloat16)).astype(jnp.float32)
-    return (residual.astype(jnp.float32) + summed_down).astype(jnp.bfloat16)
+    return scatter_added(down_terms.astype(jnp.bfloat16), residual, 4)
 
 
 def solution(mesh):
@@ -248,7 +498,7 @@
     owners = mesh.shape["fs"] * mesh.shape["tp"]
 
     def run(*arrays):
-        owned = arrays[6].shape[0] % owners == 0
+        owned = arrays[6].shape[0] % owners == 0 and mesh.shape["tp"] == 4
         body = per_device_owned if owned else per_device
         return jax.shard_map(
             body, mesh=mesh, in_specs=placed, out_specs=P(("grp", "fs"), "tp"), check_vma=False

time: 571 us -> 273 us (0.48)
  waiting for transfers between devices: 241 us -> 4.43 us
  local copies, waits for them, and re-layouts: 220 us -> 57.4 us
  Pallas kernels: 0 us -> 147 us
  other arithmetic: 23.7 us -> 1.33 us
  between operations: 14.8 us -> 0.54 us
    reduce_scatter x4 -> x0, waiting for transfers between devices: 150 us -> none  [the longest x2 91.3 us: scatter_sum(): partials = lax.psum_scatter(partials, 'tp', scatter_dimension=1, tiled=True)]
    pallas_call x0 -> x5, Pallas kernels: none -> 147 us  [the longest x2 72.5 us: gather_normed(): pl.pallas_call(functools.partial(gather_kernel, count), out_shape=jax.Sha...]
    slice x43 -> x0, local copies, waits for them, and re-layouts: 122 us -> none  [recurrent_state(): _, hidden = lax.associative_scan(combine, (decay, drive), axis=0)]
    all_gather x4 -> x0, waiting for transfers between devices: 59 us -> none  [the longest x2 58.9 us: gather_all(): rows = lax.all_gather(rows, 'fs', axis=0, tiled=True)]
    pad x14 -> x0, local copies, waits for them, and re-layouts: 38 us -> none  [recurrent_state(): _, hidden = lax.associative_scan(combine, (decay, drive), axis=0)]
    ppermute x15 -> x12, waiting for transfers between devices: 30.5 us -> 0.03 us  [exchange_blocks(): lax.ppermute(part, 'fs', [(i, (i + step) % count) for i in range(count)])]
    add x20 -> x0, other arithmetic: 8.44 us -> none  [the longest x13 8.12 us: combine(): return (earlier[0] * later[0], later[0] * earlier[1] + later[1])]
    reduce_sum x2 -> x0, other arithmetic: 6.3 us -> none  [rms_rows(): jnp.mean(values * values, axis=-1, keepdims=True) + 1e-06]
  transfers between devices with their start and end apart: 38 -> 24, of which waited for: 11 -> 2; matrix products, arithmetic and copies ran while one was open for 9% -> 21% of each run, Pallas kernels for 0% -> 40%
where the time goes in v2:
time: 273 us; the launch traced here: 271 us
  Pallas kernels  147 us (54%)
  local copies, waits for them, and re-layouts  57.4 us (21%)
  starting transfers between devices  34.2 us (13%)
  matrix products  14.1 us (5%)
  blocking collectives  12.9 us (5%)
  waiting for transfers between devices  4.43 us (2%)
    pallas_call x2, Pallas kernels, gather_normed(): pl.pallas_call(functools.partial(gather_kernel, count), out_shape=jax.Sha...  72.5 us
    pallas_call x2, Pallas kernels, scatter_added(): pl.pallas_call(functools.partial(scatter_kernel, count), out_shape=jax.Sh...  72.1 us
    dynamic_update_slice x28, local copies, waits for them, and re-layouts, put(): return lax.dynamic_update_slice(joined, value, place)  42.6 us
    ppermute x12, starting transfers between devices, exchange_blocks(): lax.ppermute(part, 'fs', [(i, (i + step) % count) for i in range(count)])  19.2 us
    ppermute x12, starting transfers between devices, exchange_blocks(): lax.ppermute(part, 'grp', [(i, (i + turn) % planes) for i in range(planes)])  15 us
    all_gather x1, blocking collectives, per_device_owned(): extra = lax.all_gather(extra_log_decay, 'fs', axis=0, tiled=True)  12.9 us
    dot_general x1, matrix products, per_device_owned(): jnp.dot(squared, down_weight, preferred_element_type=jnp.float32)  9.42 us
  transfers between devices with their start and end apart: 24, of which 2 were waited for; matrix products, arithmetic and copies ran while one was open for 21% of the time, Pallas kernels for 40%

profile of v2, /device:TPU:0, one launch (start us, length us, event | category | flops | bytes accessed | tf_op | source)
XLA Modules:
  0.0 271.5 jit_solution(18050161316955488796)
XLA Ops:
  0.0 1.7 constant_dynamic-slice_fusion.2
  1.7 5.1 %collective-permute-start.10 = (bf16[64,512]{1,0:T(8,128)(2,1)}, bf16[64,512]{1,0:T(8,128)(2,1)}, u32[]{:S(2)}, u32[]{:S(2)}) collective-permute-start(bf16[64,512]{1,0:T(8,128)(2,1)} %get-tuple-element.14), channel_id=1, source_target_pairs={{0,12},{4,0},{8,4},{12,8},{1,13},{5,1},{9,5},{13,9},{2,14},{6,2},{... | collective-permute-start | bytes 196616 | tf_op jit(solution)/shard_map/ppermute | solution.py:161
  6.8 1.0 collective-permute-start.8
  7.8 1.2 reshape.22
  8.9 1.2 reshape.23
  10.1 0.6 pad_maximum_fusion
  10.9 1.0 fusion.4
  11.9 1.9 collective-permute-start.2
  13.8 1.5 collective-permute-start
  15.3 1.4 fusion.3
  16.7 1.5 broadcast_in_dim.14
  18.2 0.9 dynamic-slice_dynamic-update-slice_fusion.1
  19.1 1.1 dynamic-slice_dynamic-update-slice_fusion.3
  20.9 0.8 constant_dynamic-slice_fusion.6
  21.9 0.8 fusion.1.rate_ref
  22.7 1.6 collective-permute-start.11
  24.8 1.5 collective-permute-start.9
  26.8 37.3 %shard_map.127 = bf16[1024,2048]{1,0:T(8,128)(2,1)S(1)} custom-call(bf16[256,512]{1,0:T(8,128)(2,1)S(1)} %copy-done.4, f32[1,2048]{1,0:T(1,128)S(1)} %bitcast.15), custom_call_target="tpu_custom_call" | custom-call | flops 1000000000 | bytes 100000000 | tf_op jit(solution)/shard_map/pallas_call | solution.py:253
  64.1 2.0 copy-done.2
  66.1 12.9 %all-gather = f32[4,1,256]{2,1,0:T(1,128)S(1)} all-gather(f32[1,1,256]{2,1,0:T(1,128)S(1)} %bitcast.21), channel_id=1, replica_groups=mesh['grp'=2,'fs'=4,'tp'=4] {'fs'}, dimensions={0}, use_global_device_ids=true | all-gather | bytes 5120 | tf_op jit(solution)/shard_map/all_gather | solution.py:459
  79.3 2.3 dynamic_update_slice.92
  81.7 2.1 dynamic_update_slice.93
  83.8 2.6 dynamic_update_slice.94
  86.4 1.4 collective-permute-start.16
  87.9 2.1 dynamic_update_slice.95
  90.0 2.6 dynamic_update_slice.96
  92.6 0.6 collective-permute-start.12
  93.2 2.1 dynamic_update_slice.97
  95.3 0.9 constant_dynamic-update-slice_fusion.11
  96.2 1.1 collective-permute-start.14
  97.4 1.7 collective-permute-start.3
  99.1 3.1 %collective-permute-start.22 = (bf16[256,512]{1,0:T(8,128)(2,1)S(1)}, bf16[256,512]{1,0:T(8,128)(2,1)S(1)}, u32[]{:S(2)}, u32[]{:S(2)}) collective-permute-start(bf16[256,512]{1,0:T(8,128)(2,1)S(1)} %get-tuple-element.8), channel_id=1, source_target_pairs={{0,12},{4,0},{8,4},{12,8},{1,13},{5,1},{9,5},{13,9},{2,14},{6,2},{... | collective-permute-start | bytes 786440 | tf_op jit(solution)/shard_map/ppermute | solution.py:161
  102.2 1.2 collective-permute-done.3
  103.4 1.7 collective-permute-start.5
  105.2 3.2 %collective-permute-done.5 = bf16[256,256]{1,0:T(8,128)(2,1)S(1)} collective-permute-done((bf16[256,256]{1,0:T(8,128)(2,1)S(1)}, bf16[256,256]{1,0:T(8,128)(2,1)S(1)}, u32[]{:S(2)}, u32[]{:S(2)}) %collective-permute-start.5) | collective-permute-done | bytes 131104 | tf_op jit(solution)/shard_map/ppermute | solution.py:164
  108.4 2.6 collective-permute-start.18
  111.0 3.4 %fusion.5.gate_ref.recur_ref = f32[1024,256]{1,0:T(8,128)S(1)} fusion(bf16[1024,2048]{1,0:T(8,128)(2,1)} %copy-done.2, bf16[2048,256]{1,0:T(8,128)(2,1)S(1)} %constant_dynamic-update-slice_fusion.6), kind=kOutput, calls=%fused_computation.35 | convolution fusion | flops 1073741824 | bytes 6291456 | tf_op jit(solution)/shard_map/dot_general | solution.py:463
  114.5 2.0 shard_map.128
  116.5 0.9 collective-permute-start.20
  117.4 1.2 convolution_convert_fusion.1.terms_ref
  118.6 1.8 collective-permute-start.13
  120.4 34.0 %shard_map.129.own_ref.base_ref = bf16[256,512]{1,0:T(8,128)(2,1)S(1)} custom-call(bf16[1024,2048]{1,0:T(8,128)(2,1)S(1)} %convolution_convert_fusion.1.terms_ref, bf16[256,512]{1,0:T(8,128)(2,1)S(1)} %copy-done.4), custom_call_target="tpu_custom_call" | custom-call | flops 1000000000 | bytes 100000000 | tf_op jit(solution)/shard_map/pallas_call | solution.py:356
  154.5 0.7 constant_dynamic-update-slice_fusion.5
  155.2 1.2 collective-permute-start.15
  156.5 0.8 collective-permute-start.23
  157.2 1.2 collective-permute-start.19
  158.5 0.8 collective-permute-start.21
  159.3 35.2 %shard_map.130 = bf16[1024,2048]{1,0:T(8,128)(2,1)S(1)} custom-call(bf16[256,512]{1,0:T(8,128)(2,1)S(1)} %shard_map.129.own_ref.base_ref, f32[1,2048]{1,0:T(1,128)S(1)} %bitcast.16), custom_call_target="tpu_custom_call" | custom-call | flops 1000000000 | bytes 100000000 | tf_op jit(solution)/shard_map/pallas_call | solution.py:253
  194.5 3.0 %dynamic_update_slice.106 = bf16[512,2048]{1,0:T(8,128)(2,1)S(1)} dynamic-update-slice(bf16[512,2048]{1,0:T(8,128)(2,1)S(1)} %copy-done.8, bf16[256,512]{1,0:T(8,128)(2,1)S(1)} %collective-permute-done.18, s32[]{:T(128)S(6)} %select_n.146, s32[]{:T(128)S(6)} %select_n.167) | dynamic-update-slice | bytes 524292 | tf_op jit(solution)/shard_map/dynamic_update_slice | solution.py:153
  197.5 1.5 collective-permute-start.17
  199.1 0.7 constant_dynamic-update-slice_fusion.4
  199.8 0.7 constant_dynamic-update-slice_fusion.3
  200.5 2.5 dynamic_update_slice.107
  203.0 4.4 %dynamic_update_slice.108 = bf16[512,2048]{1,0:T(8,128)(2,1)S(1)} dynamic-update-slice(bf16[512,2048]{1,0:T(8,128)(2,1)S(1)} %dynamic_update_slice.107, bf16[256,512]{1,0:T(8,128)(2,1)S(1)} %collective-permute-done.20, s32[]{:T(128)S(6)} %select_n.146, s32[]{:T(128)S(6)} %select_n.171) | dynamic-update-slice | bytes 524292 | tf_op jit(solution)/shard_map/dynamic_update_slice | solution.py:153
  207.4 3.5 %dynamic_update_slice.109 = bf16[512,2048]{1,0:T(8,128)(2,1)S(1)} dynamic-update-slice(bf16[512,2048]{1,0:T(8,128)(2,1)S(1)} %dynamic_update_slice.108, bf16[256,512]{1,0:T(8,128)(2,1)S(1)} %collective-permute-done.21, s32[]{:T(128)S(6)} %select_n.178, s32[]{:T(128)S(6)} %select_n.171) | dynamic-update-slice | bytes 524292 | tf_op jit(solution)/shard_map/dynamic_update_slice | solution.py:153
  210.8 4.4 %dynamic_update_slice.110 = bf16[512,2048]{1,0:T(8,128)(2,1)S(1)} dynamic-update-slice(bf16[512,2048]{1,0:T(8,128)(2,1)S(1)} %dynamic_update_slice.109, bf16[256,512]{1,0:T(8,128)(2,1)S(1)} %collective-permute-done.22, s32[]{:T(128)S(6)} %select_n.146, s32[]{:T(128)S(6)} %select_n.174) | dynamic-update-slice | bytes 524292 | tf_op jit(solution)/shard_map/dynamic_update_slice | solution.py:153
  215.2 3.7 %dynamic_update_slice.111 = bf16[512,2048]{1,0:T(8,128)(2,1)S(1)} dynamic-update-slice(bf16[512,2048]{1,0:T(8,128)(2,1)S(1)} %dynamic_update_slice.110, bf16[256,512]{1,0:T(8,128)(2,1)S(1)} %collective-permute-done.23, s32[]{:T(128)S(6)} %select_n.178, s32[]{:T(128)S(6)} %select_n.174) | dynamic-update-slice | bytes 524292 | tf_op jit(solution)/shard_map/dynamic_update_slice | solution.py:153
  219.0 0.7 constant_dynamic-update-slice_fusion.2
  219.7 0.7 constant_dynamic-update-slice_fusion.1
  220.4 0.7 constant_dynamic-update-slice_fusion
  221.1 9.4 %convolution_convert_fusion.terms_ref = bf16[1024,2048]{1,0:T(8,128)(2,1)} fusion(bf16[512,2048]{1,0:T(8,128)(2,1)S(1)} %dynamic_update_slice.111, bf16[1024,2048]{1,0:T(8,128)(2,1)} %copy-done.3, bf16[2048,512]{1,0:T(8,128)(2,1)} %constant_dynamic-update-slice_fusion), kind=kOutput, calls=%fused_computation | convolution fusion | flops 4298637312 | bytes 12582912 | tf_op jit(solution)/shard_map/dot_general | solution.py:478
  230.6 2.2 copy-done.1
  232.7 38.0 %shard_map.131 = bf16[256,512]{1,0:T(8,128)(2,1)S(1)} custom-call(bf16[1024,2048]{1,0:T(8,128)(2,1)S(1)} %copy-done.1, bf16[256,512]{1,0:T(8,128)(2,1)S(1)} %shard_map.129.own_ref.base_ref), custom_call_target="tpu_custom_call" | custom-call | flops 1000000000 | bytes 100000000 | tf_op jit(solution)/shard_map/pallas_call | solution.py:356
  270.8 0.7 copy.46
  (62 shorter events, 2.5 us)
Async XLA Ops:
  0.0 21.9 %copy-start = (bf16[4,512]{1,0:T(4,128)(2,1)S(1)}, bf16[4,512]{1,0:T(4,128)(2,1)}, u32[]{:S(2)}) copy-start(bf16[4,512]{1,0:T(4,128)(2,1)} %param.18) | copy-start | bytes 12292
  1.7 21.0 %collective-permute-start.10 = (bf16[64,512]{1,0:T(8,128)(2,1)}, bf16[64,512]{1,0:T(8,128)(2,1)}, u32[]{:S(2)}, u32[]{:S(2)}) collective-permute-start(bf16[64,512]{1,0:T(8,128)(2,1)} %get-tuple-element.14), channel_id=1, source_target_pairs={{0,12},{4,0},{8,4},{12,8},{1,13},{5,1},{9,5},{13,9},{2,14},{6,2},{... | collective-permute-start | bytes 196616 | tf_op jit(solution)/shard_map/ppermute | solution.py:161
  6.8 17.5 %collective-permute-start.6 = (bf16[64,512]{1,0:T(8,128)(2,1)}, bf16[64,512]{1,0:T(8,128)(2,1)}, u32[]{:S(2)}, u32[]{:S(2)}) collective-permute-start(bf16[64,512]{1,0:T(8,128)(2,1)} %get-tuple-element.15), channel_id=1, source_target_pairs={{0,4},{4,8},{8,12},{12,0},{1,5},{5,9},{9,13},{13,1},{2,6},{6,10},{... | collective-permute-start | bytes 196616 | tf_op jit(solution)/shard_map/ppermute | solution.py:161
  6.8 18.0 %collective-permute-start.8 = (bf16[64,512]{1,0:T(8,128)(2,1)}, bf16[64,512]{1,0:T(8,128)(2,1)}, u32[]{:S(2)}, u32[]{:S(2)}) collective-permute-start(bf16[64,512]{1,0:T(8,128)(2,1)} %get-tuple-element.16), channel_id=1, source_target_pairs={{0,8},{4,12},{8,0},{12,4},{1,9},{5,13},{9,1},{13,5},{2,10},{6,14},... | collective-permute-start | bytes 196616 | tf_op jit(solution)/shard_map/ppermute | solution.py:161
  10.1 5.2 %copy-start.9 = (bf16[512,2048]{1,0:T(8,128)(2,1)S(1)}, bf16[512,2048]{1,0:T(8,128)(2,1)}, u32[]{:S(2)}) copy-start(bf16[512,2048]{1,0:T(8,128)(2,1)} %param.24) | copy-start | bytes 6291460
  11.9 84.3 %collective-permute-start.2 = (bf16[256,256]{1,0:T(8,128)(2,1)}, bf16[256,256]{1,0:T(8,128)(2,1)S(1)}, u32[]{:S(2)}, u32[]{:S(2)}) collective-permute-start(bf16[256,256]{1,0:T(8,128)(2,1)} %get-tuple-element.12), channel_id=1, source_target_pairs={{0,8},{4,12},{8,0},{12,4},{1,9},{5,13},{9,1},{13,5},{2,10},{6,14},... | collective-permute-start | bytes 393224 | tf_op jit(solution)/shard_map/ppermute | solution.py:161
  13.8 12.5 %collective-permute-start = (bf16[256,256]{1,0:T(8,128)(2,1)}, bf16[256,256]{1,0:T(8,128)(2,1)}, u32[]{:S(2)}, u32[]{:S(2)}) collective-permute-start(bf16[256,256]{1,0:T(8,128)(2,1)} %get-tuple-element.13), channel_id=1, source_target_pairs={{0,4},{4,8},{8,12},{12,0},{1,5},{5,9},{9,13},{13,1},{2,6},{6,10},{... | collective-permute-start | bytes 393224 | tf_op jit(solution)/shard_map/ppermute | solution.py:161
  19.1 1.7 copy-start.10
  20.3 6.5 %copy-start.4 = (bf16[256,512]{1,0:T(8,128)(2,1)S(1)}, bf16[256,512]{1,0:T(8,128)(2,1)}, u32[]{:S(2)}) copy-start(bf16[256,512]{1,0:T(8,128)(2,1)} %base_ref.1) | copy-start | bytes 786436
  20.4 6.5 %copy-start.5 = (f32[2048]{0:T(1024)S(1)}, f32[2048]{0:T(1024)}, u32[]{:S(2)}) copy-start(f32[2048]{0:T(1024)} %param.14) | copy-start | bytes 24580
  20.9 6.0 %copy-start.7 = (bf16[512,2048]{1,0:T(8,128)(2,1)}, bf16[512,2048]{1,0:T(8,128)(2,1)S(1)}, u32[]{:S(2)}) copy-start(bf16[512,2048]{1,0:T(8,128)(2,1)S(1)} %dynamic-slice_dynamic-update-slice_fusion) | copy-start | bytes 6291460
  22.7 69.9 %collective-permute-start.11 = (bf16[64,512]{1,0:T(8,128)(2,1)}, bf16[64,512]{1,0:T(8,128)(2,1)}, u32[]{:S(2)}, u32[]{:S(2)}) collective-permute-start(bf16[64,512]{1,0:T(8,128)(2,1)} %collective-permute-done.10), channel_id=1, source_target_pairs={{0,16},{16,0},{1,17},{17,1},{2,18},{18,2},{3,19},{19,3},{4,20},{20... | collective-permute-start | bytes 196616 | tf_op jit(solution)/shard_map/ppermute | solution.py:164
  24.3 57.4 %collective-permute-start.7 = (bf16[64,512]{1,0:T(8,128)(2,1)}, bf16[64,512]{1,0:T(8,128)(2,1)}, u32[]{:S(2)}, u32[]{:S(2)}) collective-permute-start(bf16[64,512]{1,0:T(8,128)(2,1)} %collective-permute-done.6), channel_id=1, source_target_pairs={{0,16},{16,0},{1,17},{17,1},{2,18},{18,2},{3,19},{19,3},{4,20},{20... | collective-permute-start | bytes 196616 | tf_op jit(solution)/shard_map/ppermute | solution.py:164
  24.8 61.6 %collective-permute-start.9 = (bf16[64,512]{1,0:T(8,128)(2,1)}, bf16[64,512]{1,0:T(8,128)(2,1)}, u32[]{:S(2)}, u32[]{:S(2)}) collective-permute-start(bf16[64,512]{1,0:T(8,128)(2,1)} %collective-permute-done.8), channel_id=1, source_target_pairs={{0,16},{16,0},{1,17},{17,1},{2,18},{18,2},{3,19},{19,3},{4,20},{20... | collective-permute-start | bytes 196616 | tf_op jit(solution)/shard_map/ppermute | solution.py:164
  26.3 71.0 %collective-permute-start.1 = (bf16[256,256]{1,0:T(8,128)(2,1)}, bf16[256,256]{1,0:T(8,128)(2,1)S(1)}, u32[]{:S(2)}, u32[]{:S(2)}) collective-permute-start(bf16[256,256]{1,0:T(8,128)(2,1)} %collective-permute-done), channel_id=1, source_target_pairs={{0,16},{16,0},{1,17},{17,1},{2,18},{18,2},{3,19},{19,3},{4,20},{20... | collective-permute-start | bytes 393224 | tf_op jit(solution)/shard_map/ppermute | solution.py:164
  26.8 39.3 %copy-start.11 = (f32[256]{0:T(256)S(1)}, f32[256]{0:T(256)}, u32[]{:S(2)}) copy-start(f32[256]{0:T(256)} %param.22) | copy-start | bytes 3076
  64.1 2.0 copy-start.2
  81.7 17.4 %collective-permute-start.4 = (bf16[256,256]{1,0:T(8,128)(2,1)}, bf16[256,256]{1,0:T(8,128)(2,1)S(1)}, u32[]{:S(2)}, u32[]{:S(2)}) collective-permute-start(bf16[256,256]{1,0:T(8,128)(2,1)} %get-tuple-element.11), channel_id=1, source_target_pairs={{0,12},{4,0},{8,4},{12,8},{1,13},{5,1},{9,5},{13,9},{2,14},{6,2},{... | collective-permute-start | bytes 393224 | tf_op jit(solution)/shard_map/ppermute | solution.py:161
  86.4 30.1 %collective-permute-start.16 = (bf16[256,512]{1,0:T(8,128)(2,1)}, bf16[256,512]{1,0:T(8,128)(2,1)S(1)}, u32[]{:S(2)}, u32[]{:S(2)}) collective-permute-start(bf16[256,512]{1,0:T(8,128)(2,1)} %get-tuple-element.5), channel_id=1, source_target_pairs={{0,12},{4,0},{8,4},{12,8},{1,13},{5,1},{9,5},{13,9},{2,14},{6,2},{... | collective-permute-start | bytes 786440 | tf_op jit(solution)/shard_map/ppermute | solution.py:161
  92.6 26.0 %collective-permute-start.12 = (bf16[256,512]{1,0:T(8,128)(2,1)}, bf16[256,512]{1,0:T(8,128)(2,1)S(1)}, u32[]{:S(2)}, u32[]{:S(2)}) collective-permute-start(bf16[256,512]{1,0:T(8,128)(2,1)} %get-tuple-element.6), channel_id=1, source_target_pairs={{0,4},{4,8},{8,12},{12,0},{1,5},{5,9},{9,13},{13,1},{2,6},{6,10},{... | collective-permute-start | bytes 786440 | tf_op jit(solution)/shard_map/ppermute | solution.py:161
  96.2 59.0 %collective-permute-start.14 = (bf16[256,512]{1,0:T(8,128)(2,1)}, bf16[256,512]{1,0:T(8,128)(2,1)S(1)}, u32[]{:S(2)}, u32[]{:S(2)}) collective-permute-start(bf16[256,512]{1,0:T(8,128)(2,1)} %get-tuple-element.7), channel_id=1, source_target_pairs={{0,8},{4,12},{8,0},{12,4},{1,9},{5,13},{9,1},{13,5},{2,10},{6,14},... | collective-permute-start | bytes 786440 | tf_op jit(solution)/shard_map/ppermute | solution.py:161
  97.4 6.1 %collective-permute-start.3 = (bf16[256,256]{1,0:T(8,128)(2,1)S(1)}, bf16[256,256]{1,0:T(8,128)(2,1)S(1)}, u32[]{:S(2)}, u32[]{:S(2)}) collective-permute-start(bf16[256,256]{1,0:T(8,128)(2,1)S(1)} %collective-permute-done.2), channel_id=1, source_target_pairs={{0,16},{16,0},{1,17},{17,1},{2,18},{18,2},{3,19},{19,3},{4,20},{20... | collective-permute-start | bytes 393224 | tf_op jit(solution)/shard_map/ppermute | solution.py:164
  99.1 57.3 %collective-permute-start.22 = (bf16[256,512]{1,0:T(8,128)(2,1)S(1)}, bf16[256,512]{1,0:T(8,128)(2,1)S(1)}, u32[]{:S(2)}, u32[]{:S(2)}) collective-permute-start(bf16[256,512]{1,0:T(8,128)(2,1)S(1)} %get-tuple-element.8), channel_id=1, source_target_pairs={{0,12},{4,0},{8,4},{12,8},{1,13},{5,1},{9,5},{13,9},{2,14},{6,2},{... | collective-permute-start | bytes 786440 | tf_op jit(solution)/shard_map/ppermute | solution.py:161
  103.4 5.0 %collective-permute-start.5 = (bf16[256,256]{1,0:T(8,128)(2,1)S(1)}, bf16[256,256]{1,0:T(8,128)(2,1)S(1)}, u32[]{:S(2)}, u32[]{:S(2)}) collective-permute-start(bf16[256,256]{1,0:T(8,128)(2,1)S(1)} %collective-permute-done.4), channel_id=1, source_target_pairs={{0,16},{16,0},{1,17},{17,1},{2,18},{18,2},{3,19},{19,3},{4,20},{20... | collective-permute-start | bytes 393224 | tf_op jit(solution)/shard_map/ppermute | solution.py:164
  108.4 48.8 %collective-permute-start.18 = (bf16[256,512]{1,0:T(8,128)(2,1)S(1)}, bf16[256,512]{1,0:T(8,128)(2,1)S(1)}, u32[]{:S(2)}, u32[]{:S(2)}) collective-permute-start(bf16[256,512]{1,0:T(8,128)(2,1)S(1)} %get-tuple-element.9), channel_id=1, source_target_pairs={{0,4},{4,8},{8,12},{12,0},{1,5},{5,9},{9,13},{13,1},{2,6},{6,10},{... | collective-permute-start | bytes 786440 | tf_op jit(solution)/shard_map/ppermute | solution.py:161
  116.5 42.0 %collective-permute-start.20 = (bf16[256,512]{1,0:T(8,128)(2,1)S(1)}, bf16[256,512]{1,0:T(8,128)(2,1)S(1)}, u32[]{:S(2)}, u32[]{:S(2)}) collective-permute-start(bf16[256,512]{1,0:T(8,128)(2,1)S(1)} %get-tuple-element.10), channel_id=1, source_target_pairs={{0,8},{4,12},{8,0},{12,4},{1,9},{5,13},{9,1},{13,5},{2,10},{6,14},... | collective-permute-start | bytes 786440 | tf_op jit(solution)/shard_map/ppermute | solution.py:161
  118.6 40.7 %copy-start.6 = (f32[2048]{0:T(1024)S(1)}, f32[2048]{0:T(1024)}, u32[]{:S(2)}) copy-start(f32[2048]{0:T(1024)} %param.15) | copy-start | bytes 24580
  118.6 78.9 %collective-permute-start.13 = (bf16[256,512]{1,0:T(8,128)(2,1)S(1)}, bf16[256,512]{1,0:T(8,128)(2,1)S(1)}, u32[]{:S(2)}, u32[]{:S(2)}) collective-permute-start(bf16[256,512]{1,0:T(8,128)(2,1)S(1)} %collective-permute-done.12), channel_id=1, source_target_pairs={{0,16},{16,0},{1,17},{17,1},{2,18},{18,2},{3,19},{19,3},{4,20},{20... | collective-permute-start | bytes 786440 | tf_op jit(solution)/shard_map/ppermute | solution.py:164
  155.2 63.7 %collective-permute-start.15 = (bf16[256,512]{1,0:T(8,128)(2,1)S(1)}, bf16[256,512]{1,0:T(8,128)(2,1)S(1)}, u32[]{:S(2)}, u32[]{:S(2)}) collective-permute-start(bf16[256,512]{1,0:T(8,128)(2,1)S(1)} %collective-permute-done.14), channel_id=1, source_target_pairs={{0,16},{16,0},{1,17},{17,1},{2,18},{18,2},{3,19},{19,3},{4,20},{20... | collective-permute-start | bytes 786440 | tf_op jit(solution)/shard_map/ppermute | solution.py:164
  156.5 58.8 %collective-permute-start.23 = (bf16[256,512]{1,0:T(8,128)(2,1)S(1)}, bf16[256,512]{1,0:T(8,128)(2,1)S(1)}, u32[]{:S(2)}, u32[]{:S(2)}) collective-permute-start(bf16[256,512]{1,0:T(8,128)(2,1)S(1)} %collective-permute-done.22), channel_id=1, source_target_pairs={{0,16},{16,0},{1,17},{17,1},{2,18},{18,2},{3,19},{19,3},{4,20},{20... | collective-permute-start | bytes 786440 | tf_op jit(solution)/shard_map/ppermute | solution.py:164
  157.2 43.3 %collective-permute-start.19 = (bf16[256,512]{1,0:T(8,128)(2,1)S(1)}, bf16[256,512]{1,0:T(8,128)(2,1)S(1)}, u32[]{:S(2)}, u32[]{:S(2)}) collective-permute-start(bf16[256,512]{1,0:T(8,128)(2,1)S(1)} %collective-permute-done.18), channel_id=1, source_target_pairs={{0,16},{16,0},{1,17},{17,1},{2,18},{18,2},{3,19},{19,3},{4,20},{20... | collective-permute-start | bytes 786440 | tf_op jit(solution)/shard_map/ppermute | solution.py:164
  158.5 48.9 %collective-permute-start.21 = (bf16[256,512]{1,0:T(8,128)(2,1)S(1)}, bf16[256,512]{1,0:T(8,128)(2,1)S(1)}, u32[]{:S(2)}, u32[]{:S(2)}) collective-permute-start(bf16[256,512]{1,0:T(8,128)(2,1)S(1)} %collective-permute-done.20), channel_id=1, source_target_pairs={{0,16},{16,0},{1,17},{17,1},{2,18},{18,2},{3,19},{19,3},{4,20},{20... | collective-permute-start | bytes 786440 | tf_op jit(solution)/shard_map/ppermute | solution.py:164
  159.3 35.2 %copy-start.8 = (bf16[512,2048]{1,0:T(8,128)(2,1)S(1)}, bf16[512,2048]{1,0:T(8,128)(2,1)}, u32[]{:S(2)}) copy-start(bf16[512,2048]{1,0:T(8,128)(2,1)} %copy-done.7) | copy-start | bytes 6291460
  194.5 24.4 %copy-start.3 = (bf16[1024,2048]{1,0:T(8,128)(2,1)}, bf16[1024,2048]{1,0:T(8,128)(2,1)S(1)}, u32[]{:S(2)}) copy-start(bf16[1024,2048]{1,0:T(8,128)(2,1)S(1)} %shard_map.130) | copy-start | bytes 12582916
  197.5 22.9 %collective-permute-start.17 = (bf16[256,512]{1,0:T(8,128)(2,1)S(1)}, bf16[256,512]{1,0:T(8,128)(2,1)S(1)}, u32[]{:S(2)}, u32[]{:S(2)}) collective-permute-start(bf16[256,512]{1,0:T(8,128)(2,1)S(1)} %collective-permute-done.16), channel_id=1, source_target_pairs={{0,16},{16,0},{1,17},{17,1},{2,18},{18,2},{3,19},{19,3},{4,20},{20... | collective-permute-start | bytes 786440 | tf_op jit(solution)/shard_map/ppermute | solution.py:164
  230.6 2.2 copy-start.1

commit v3 on v2

--- a/solution.py
+++ b/solution.py
@@ -132,41 +132,6 @@
     return (residual.astype(jnp.float32) + summed_down).astype(jnp.bfloat16)
 
 
-def exchange_blocks(weight, split_axis, join_axis):
-    count, mine = lax.axis_size("fs"), lax.axis_index("fs")
-    planes, plane = lax.axis_size("grp"), lax.axis_index("grp")
-    width = weight.shape[split_axis] // count
-    depth = weight.shape[join_axis]
-
-    def piece(owner):
-        return lax.dynamic_slice_in_dim(weight, owner * width, width, split_axis)
-
-    shape = list(weight.shape)
-    shape[split_axis] = width
-    shape[join_axis] = depth * count
-    joined = jnp.zeros(shape, weight.dtype)
-
-    def put(joined, value, row, column):
-        place = [0, 0]
-        place[join_axis] += column
-        place[0] = place[0] + row
-        return lax.dynamic_update_slice(joined, value, place)
-
-    joined = put(joined, piece(mine), 0, mine * depth)
-    share = (depth if join_axis == 0 else width) // planes
-    for step in range(1, count):
-        target = lax.rem(mine + step, count)
-        source = lax.rem(mine - step + count, count)
-        part = lax.dynamic_slice_in_dim(piece(target), plane * share, share, 0)
-        part = lax.ppermute(part, "fs", [(i, (i + step) % count) for i in range(count)])
-        joined = put(joined, part, plane * share, source * depth)
-        for turn in range(1, planes):
-            other = lax.ppermute(part, "grp", [(i, (i + turn) % planes) for i in range(planes)])
-            origin = lax.rem(plane - turn + planes, planes)
-            joined = put(joined, other, origin * share, source * depth)
-    return joined
-
-
 def steps_by_distance(count):
     return sorted(range(1, count), key=lambda step: (min(step, count - step), step))
 
@@ -174,13 +139,101 @@
 def greet(count, place, row):
     barrier = pltpu.get_barrier_semaphore()
     peers = [{"fs": lax.rem(place + step, count)} for step in range(1, count)]
-    peers += [{"tp": row ^ 1}, {"tp": row ^ 2}]
+    peers += [{"tp": row ^ 1}, {"tp": row ^ 2}, {"grp": 1 - lax.axis_index("grp")}]
     for peer in peers:
         pl.semaphore_signal(barrier, inc=1, device_id=peer, device_id_type=MESH)
     pl.semaphore_wait(barrier, len(peers))
 
 
-def gather_kernel(count, own_ref, gain_ref, out_ref, held, send_z, send_x, send_c, arrived):
+class Exchange:
+    def __init__(self, count, axis, weight, joined, sems):
+        self.count, self.axis, self.weight, self.joined, self.sems = (
+            count, axis, weight, joined, sems
+        )
+        self.place, self.plane = lax.axis_index("fs"), lax.axis_index("grp")
+        self.width = weight.shape[axis] // count
+        self.depth = weight.shape[1 - axis]
+        self.share = (self.depth if axis else self.width) // 2
+        self.order = steps_by_distance(count)
+        self.started = []
+
+    def spot(self, rows, columns, row_step, column_step):
+        return (
+            pl.ds(pl.multiple_of(rows, row_step), self.share),
+            pl.ds(pl.multiple_of(columns, column_step), self.width if self.axis else self.depth),
+        )
+
+    def leaving(self, owner, plane):
+        half = plane * self.share
+        if self.axis:
+            return self.spot(half, owner * self.width, self.share, self.width)
+        return self.spot(owner * self.width + half, 0, self.share, self.depth)
+
+    def landing(self, source, plane):
+        half = plane * self.share
+        if self.axis:
+            return self.spot(source * self.depth + half, 0, self.share, self.width)
+        return self.spot(half, source * self.depth, self.share, self.depth)
+
+    def copy(self, source, target, stage, step, peer):
+        return pltpu.make_async_remote_copy(
+            src_ref=source,
+            dst_ref=target,
+            send_sem=self.sems.at[stage, step],
+            recv_sem=self.sems.at[stage + 1, step],
+            device_id=peer,
+            device_id_type=MESH,
+        )
+
+    def begin(self):
+        for step in self.order:
+            owner = lax.rem(self.place + step, self.count)
+            moving = self.copy(
+                self.weight.at[self.leaving(owner, self.plane)],
+                self.joined.at[self.landing(self.place, self.plane)],
+                0, step, {"fs": owner},
+            )
+            moving.start()
+            self.started.append(moving)
+        for plane in range(2):
+            self.joined[self.landing(self.place, plane)] = self.weight[
+                self.leaving(self.place, plane)
+            ]
+
+    def forward(self, step):
+        source = lax.rem(self.place - step + self.count, self.count)
+        peer = {"grp": 1 - self.plane}
+        here = self.joined.at[self.landing(source, self.plane)]
+        self.copy(here, here, 0, step, peer).wait_recv()
+        moving = self.copy(here, here, 2, step, peer)
+        moving.start()
+        self.started.append(moving)
+
+    def finish(self):
+        for step in self.order:
+            source = lax.rem(self.place - step + self.count, self.count)
+            there = self.joined.at[self.landing(source, 1 - self.plane)]
+            self.copy(there, there, 2, step, {"grp": 1 - self.plane}).wait_recv()
+        for moving in self.started:
+            moving.wait_send()
+
+
+def joined_shape(weight, axis, count):
+    shape = list(weight.shape)
+    shape[axis] //= count
+    shape[1 - axis] *= count
+    return jax.ShapeDtypeStruct(tuple(shape), weight.dtype)
+
+
+def gather_kernel(count, axes, *refs):
+    held, send_z, send_x, send_c, arrived, moves, extra_sems = refs[-7:]
+    own_ref, gain_ref, extra_ref = refs[:3]
+    number = len(axes)
+    out_ref, extra_out = refs[3 + number : 5 + number]
+    exchanges = [
+        Exchange(count, axis, refs[3 + k], refs[5 + number + k], moves.at[k])
+        for k, axis in enumerate(axes)
+    ]
     place, row = lax.axis_index("fs"), lax.axis_index("tp")
     across, beside, corner = row ^ 2, row ^ 1, row ^ 3
     length, width = own_ref.shape
@@ -211,6 +264,21 @@
         send(own_ref, (place, row), send_z.at[step], {"fs": lax.rem(place + step, count)})
     send(own_ref, (place, row), send_x.at[0], {"tp": across})
     send(own_ref, (place, row), send_c.at[0, 0], {"tp": beside})
+    for step in order:
+        peer = lax.rem(place + step, count)
+        moving = pltpu.make_async_remote_copy(
+            src_ref=extra_ref.at[0],
+            dst_ref=extra_out.at[place],
+            send_sem=extra_sems.at[0, step],
+            recv_sem=extra_sems.at[1, step],
+            device_id={"fs": peer},
+            device_id_type=MESH,
+        )
+        moving.start()
+        started.append(moving)
+    extra_out[place] = extra_ref[0]
+    for exchange in exchanges:
+        exchange.begin()
     held[place, row] = own_ref[...]
     for step in [0] + order:
         origin = lax.rem(place - step + count, count)
@@ -221,6 +289,9 @@
             send(block, (origin, row), send_c.at[0, step], {"tp": beside})
         wait((origin, across))
         send(held.at[origin, across], (origin, across), send_c.at[1, step], {"tp": beside})
+    for exchange in exchanges:
+        for step in order:
+            exchange.forward(step)
     tile = 64
     for step in [0] + order:
         origin = lax.rem(place - step + count, count)
@@ -241,38 +312,63 @@
             return carry
 
         lax.fori_loop(0, length // tile, normalise, 0)
+    for exchange in exchanges:
+        exchange.finish()
+    for step in order:
+        there = extra_out.at[lax.rem(place - step + count, count)]
+        pltpu.make_async_remote_copy(
+            src_ref=there,
+            dst_ref=there,
+            send_sem=extra_sems.at[0, step],
+            recv_sem=extra_sems.at[1, step],
+            device_id={"tp": beside},
+            device_id_type=MESH,
+        ).wait_recv()
     for moving in started:
         moving.wait_send()
 
 
-def gather_normed(rows, norm_gain, number):
+def gather_normed(rows, norm_gain, extra, weights, axes, number):
     count = lax.axis_size("fs")
     length, width = rows.shape
     vmem = pl.BlockSpec(memory_space=pltpu.VMEM)
     dma = pltpu.SemaphoreType.DMA
     return pl.pallas_call(
-        functools.partial(gather_kernel, count),
-        out_shape=jax.ShapeDtypeStruct((count * length, 4 * width), rows.dtype),
-        in_specs=[vmem, vmem],
-        out_specs=vmem,
+        functools.partial(gather_kernel, count, axes),
+        out_shape=[
+            jax.ShapeDtypeStruct((count * length, 4 * width), rows.dtype),
+            jax.ShapeDtypeStruct((count, 1, length), extra.dtype),
+        ]
+        + [joined_shape(weight, axis, count) for weight, axis in zip(weights, axes)],
+        in_specs=[vmem] * (3 + len(axes)),
+        out_specs=[vmem] * (2 + len(axes)),
         scratch_shapes=[
             pltpu.VMEM((count, 4, length, width), rows.dtype),
             dma((count,)),
             dma((count,)),
             dma((2, count)),
             dma((count, 4)),
+            dma((len(axes), 4, count)),
+            dma((2, count)),
         ],
         compiler_params=pltpu.CompilerParams(
-            collective_id=number, has_side_effects=True, vmem_limit_bytes=24 * 2**20
+            collective_id=number, has_side_effects=True, vmem_limit_bytes=32 * 2**20
         ),
         cost_estimate=pl.CostEstimate(flops=10**9, bytes_accessed=10**8, transcendentals=0),
-    )(rows, norm_gain.reshape(1, -1))
-
-
-def scatter_kernel(
-    count, terms_ref, base_ref, out_ref,
-    from_core, to_x, from_x, to_z, from_z, send_c, recv_c, send_x, recv_x, send_z, recv_z,
-):
+    )(rows, norm_gain.reshape(1, -1), extra.reshape(1, 1, -1), *weights)
+
+
+def scatter_kernel(count, axes, *refs):
+    number = len(axes)
+    terms_ref, base_ref = refs[:2]
+    out_ref = refs[2 + number]
+    from_core, to_x, from_x, to_z, from_z, send_c, recv_c, send_x, recv_x, send_z, recv_z = refs[
+        3 + 2 * number : 14 + 2 * number
+    ]
+    exchanges = [
+        Exchange(count, axis, refs[2 + k], refs[3 + number + k], refs[-1].at[k])
+        for k, axis in enumerate(axes)
+    ]
     place, row = lax.axis_index("fs"), lax.axis_index("tp")
     across, beside, corner = row ^ 2, row ^ 1, row ^ 3
     length, width = base_ref.shape
@@ -323,6 +419,8 @@
         for side in (1, 0):
             send(*core_copy(step, side))
     wide = jnp.float32
+    for exchange in exchanges:
+        exchange.begin()
     for step in order:
         copy(*core_copy(step, 1)).wait_recv()
         mine = terms_ref[block(step, across)].astype(wide)
@@ -330,7 +428,10 @@
         send(*x_copy(step))
     total = base_ref[...].astype(wide)
     summed = None
-    for step in order:
+    for turn, step in enumerate(order):
+        if turn:
+            for exchange in exchanges:
+                exchange.forward(exchange.order[turn - 1])
         copy(*core_copy(step, 0)).wait_recv()
         copy(*x_copy(step)).wait_recv()
         mine = terms_ref[block(step, row)].astype(wide) + from_core[0, step].astype(wide)
@@ -344,29 +445,33 @@
         copy(*z_copy(step)).wait_recv()
         summed = summed + from_z[step].astype(wide)
     out_ref[...] = (total + summed).astype(out_ref.dtype)
+    for exchange in exchanges:
+        exchange.finish()
     for moving in started:
         moving.wait_send()
 
 
-def scatter_added(terms, base, number):
+def scatter_added(terms, base, weights, axes, number):
     count = lax.axis_size("fs")
     vmem = pl.BlockSpec(memory_space=pltpu.VMEM)
     dma = pltpu.SemaphoreType.DMA
     blocks = pltpu.VMEM((count,) + base.shape, base.dtype)
     return pl.pallas_call(
-        functools.partial(scatter_kernel, count),
-        out_shape=jax.ShapeDtypeStruct(base.shape, base.dtype),
-        in_specs=[vmem, vmem],
-        out_specs=vmem,
+        functools.partial(scatter_kernel, count, axes),
+        out_shape=[jax.ShapeDtypeStruct(base.shape, base.dtype)]
+        + [joined_shape(weight, axis, count) for weight, axis in zip(weights, axes)],
+        in_specs=[vmem] * (2 + len(axes)),
+        out_specs=[vmem] * (1 + len(axes)),
         scratch_shapes=[pltpu.VMEM((2, count) + base.shape, base.dtype)]
         + [blocks] * 4
         + [dma((2, count))] * 2
-        + [dma((count,))] * 4,
+        + [dma((count,))] * 4
+        + [dma((len(axes), 4, count)) for _ in axes[:1]],
         compiler_params=pltpu.CompilerParams(
             collective_id=number, has_side_effects=True, vmem_limit_bytes=24 * 2**20
         ),
         cost_estimate=pl.CostEstimate(flops=10**9, bytes_accessed=10**8, transcendentals=0),
-    )(terms, base)
+    )(terms, base, *weights)
 
 
 def recurrence_kernel(
@@ -452,13 +557,15 @@
         weight.reshape(depth, count, -1)
         for weight in (gate_projection_weight, recurrent_projection_weight)
     ]
-    both_weight = exchange_blocks(jnp.concatenate(paired, axis=2).reshape(depth, -1), 1, 0)
-    out_weight = exchange_blocks(output_projection_weight, 0, 1)
-    up_weight = exchange_blocks(up_projection_weight, 1, 0)
-    down_weight = exchange_blocks(down_projection_weight, 0, 1)
-    extra = lax.all_gather(extra_log_decay, "fs", axis=0, tiled=True)
-
-    normed = gather_normed(tokens, recurrent_norm_gain, 1)
+    paired = jnp.concatenate(paired, axis=2).reshape(depth, -1)
+    normed, extra, both_weight, out_weight = gather_normed(
+        tokens,
+        recurrent_norm_gain,
+        extra_log_decay,
+        (paired, output_projection_weight),
+        (1, 0),
+        1,
+    )
     mixed = recurrence(
         jnp.dot(normed, both_weight, preferred_element_type=jnp.float32),
         own(convolution_kernel, 1),
@@ -469,14 +576,18 @@
         count,
     )
     partials = jnp.dot(mixed, out_weight, preferred_element_type=jnp.float32)
-    residual = scatter_added(partials.astype(jnp.bfloat16), tokens, 2)
-    channel_in = gather_normed(residual, feedforward_norm_gain, 3)
+    residual, up_weight = scatter_added(
+        partials.astype(jnp.bfloat16), tokens, (up_projection_weight,), (1,), 2
+    )
+    channel_in, _, down_weight = gather_normed(
+        residual, feedforward_norm_gain, extra_log_decay, (down_projection_weight,), (0,), 3
+    )
     positive = jnp.maximum(
         jnp.dot(channel_in, up_weight, preferred_element_type=jnp.float32), 0.0
     )
     squared = (positive * positive).astype(jnp.bfloat16)
     down_terms = jnp.dot(squared, down_weight, preferred_element_type=jnp.float32)
-    return scatter_added(down_terms.astype(jnp.bfloat16), residual, 4)
+    return scatter_added(down_terms.astype(jnp.bfloat16), residual, (), (), 4)[0]
 
 
 def solution(mesh):
@@ -496,9 +607,10 @@
         P("tp", "fs"),
     )
     owners = mesh.shape["fs"] * mesh.shape["tp"]
+    fitting = mesh.shape["tp"] == 4 and mesh.shape["grp"] == 2
 
     def run(*arrays):
-        owned = arrays[6].shape[0] % owners == 0 and mesh.shape["tp"] == 4
+        owned = fitting and arrays[6].shape[0] % owners == 0
         body = per_device_owned if owned else per_device
         return jax.shard_map(
             body, mesh=mesh, in_specs=placed, out_specs=P(("grp", "fs"), "tp"), check_vma=False

time: 273 us -> 224 us (0.82)
  Pallas kernels: 147 us -> 199 us
  local copies, waits for them, and re-layouts: 57.4 us -> 11.8 us
  starting transfers between devices: 34.2 us -> 0 us
  blocking collectives: 12.9 us -> 0 us
  waiting for transfers between devices: 4.43 us -> 0 us
  matrix products: 14.1 us -> 10.8 us
    pallas_call x4, Pallas kernels: 145 us -> 197 us  [the longest x2 118 us: gather_normed(): pl.pallas_call(functools.partial(gather_kernel, count, axes), out_shape=[...]
    dynamic_update_slice x28 -> x0, local copies, waits for them, and re-layouts: 42.6 us -> none  [put(): return lax.dynamic_update_slice(joined, value, place)]
    ppermute x24 -> x0, starting transfers between devices: 34.2 us -> none  [the longest x12 19.2 us: exchange_blocks(): lax.ppermute(part, 'fs', [(i, (i + step) % count) for i in range(count)])]
    all_gather x1 -> x0, blocking collectives: 12.9 us -> none  [per_device_owned(): extra = lax.all_gather(extra_log_decay, 'fs', axis=0, tiled=True)]
    ppermute x24 -> x0, waiting for transfers between devices: 4.43 us -> none  [the longest x12 4.4 us: exchange_blocks(): lax.ppermute(part, 'grp', [(i, (i + turn) % planes) for i in range(planes)])]
    dynamic_slice x4 -> x0, local copies, waits for them, and re-layouts: 4.24 us -> none  [exchange_blocks(): part = lax.dynamic_slice_in_dim(piece(target), plane * share, share, 0)]
    unnamed x26 -> x28, local copies, waits for them, and re-layouts: 5.3 us -> 8.45 us
  transfers between devices with their start and end apart: 24 -> 0, of which waited for: 2 -> 0; matrix products, arithmetic and copies ran while one was open for 21% -> 0% of each run, Pallas kernels for 40% -> 0%
where the time goes in v3:
time: 224 us; the launch traced here: 223 us
  Pallas kernels  199 us (89%)
  local copies, waits for them, and re-layouts  11.8 us (5%)
  matrix products  10.8 us (5%)
    pallas_call x2, Pallas kernels, gather_normed(): pl.pallas_call(functools.partial(gather_kernel, count, axes), out_shape=[...  118 us
    pallas_call x2, Pallas kernels, scatter_added(): pl.pallas_call(functools.partial(scatter_kernel, count, axes), out_shape=...  79.1 us
    unnamed x28, local copies, waits for them, and re-layouts  8.45 us
    dot_general x1, matrix products, per_device_owned(): jnp.dot(squared, down_weight, preferred_element_type=jnp.float32)  8.27 us

profile of v3, /device:TPU:0, one launch (start us, length us, event | category | flops | bytes accessed | tf_op | source)
XLA Modules:
  0.0 222.9 jit_solution(4660365825304561256)
XLA Ops:
  0.0 0.0 copy-start
  0.0 0.8 fusion.1.rate_ref
  0.8 0.0 copy-done
  0.8 0.8 constant_dynamic-slice_fusion
  1.6 1.2 reshape.27
  2.8 1.2 reshape.28
  3.9 0.0 copy-start.3
  3.9 0.0 copy-start.7
  4.0 0.0 copy-start.8
  4.0 0.0 copy-start.10
  4.0 0.6 pad_maximum_fusion
  4.5 0.2 copy.15
  4.8 0.1 copy-done.3
  4.9 0.2 copy-done.7
  5.1 0.0 copy-done.8
  5.1 0.0 copy-done.10
  5.1 58.8 %shard_map.127 = (bf16[1024,2048]{1,0:T(8,128)(2,1)S(1)}, f32[4,1,256]{2,1,0:T(1,128)S(1)}, bf16[2048,256]{1,0:T(8,128)(2,1)S(1)}, bf16[128,2048]{1,0:T(8,128)(2,1)S(1)}) custom-call(bf16[256,512]{1,0:T(8,128)(2,1)S(1)} %copy-done.3, f32[1,2048]{1,0:T(1,128)S(1)} %bitcast.17, f32[1,1,256]{2,1,0:T(1,128)S(1)} %bitcast.19, bf16[512,1024]{1,0:T(8,128)(2,1)S(1)} %bitcast.15, ...), custom_call_target="tpu_custom_call" | custom-call | flops 1000000000 | bytes 100000000 | tf_op jit(solution)/shard_map/pallas_call | solution.py:336
  63.9 1.3 fusion.3.gate_ref.recur_ref
  65.2 0.2 copy.14.extra_ref
  65.4 2.0 shard_map.128
  67.4 0.0 copy-start.2
  67.4 1.2 convolution_convert_fusion.1.refs_0_
  68.7 0.3 copy-done.2
  69.0 0.0 copy-start.4
  69.0 0.0 copy-start.9
  69.0 42.5 %shard_map.129 = (bf16[256,512]{1,0:T(8,128)(2,1)S(1)}, bf16[2048,512]{1,0:T(8,128)(2,1)S(1)}) custom-call(bf16[1024,2048]{1,0:T(8,128)(2,1)S(1)} %convolution_convert_fusion.1.refs_0_, bf16[256,512]{1,0:T(8,128)(2,1)S(1)} %copy-done.3, bf16[512,2048]{1,0:T(8,128)(2,1)S(1)} %copy-done.2), custom_call_target="tpu_custom_call" | custom-call | flops 1000000000 | bytes 100000000 | tf_op jit(solution)/shard_map/pallas_call | solution.py:459
  111.5 0.0 copy-start.5
  111.5 1.3 copy-done.5
  112.9 0.0 copy-start.6
  112.9 0.0 copy-done.4
  112.9 0.0 copy-done.9
  112.9 58.9 %shard_map.130 = (bf16[1024,2048]{1,0:T(8,128)(2,1)S(1)}, f32[4,1,256]{2,1,0:T(1,128)}, bf16[512,2048]{1,0:T(8,128)(2,1)S(1)}) custom-call(bf16[256,512]{1,0:T(8,128)(2,1)S(1)} %get-tuple-element.17.refs_0_.refs_1_, f32[1,2048]{1,0:T(1,128)S(1)} %bitcast.18, f32[1,1,256]{2,1,0:T(1,128)S(1)} %bitcast.20, bf16[2048,512]{1,0:T(8,128)(2,1)S(1)} %copy-done.4), custom_call_target="tpu_custom_call" | custom-call | flops 1000000000 | bytes 100000000 | tf_op jit(solution)/shard_map/pallas_call | solution.py:336
  171.8 0.0 copy-start.11
  171.8 2.0 copy-done.11
  173.8 0.0 copy-start.12
  173.8 1.4 copy-done.12
  175.1 0.0 copy-done.6
  175.1 8.3 %convolution_convert_fusion.refs_0_ = bf16[1024,2048]{1,0:T(8,128)(2,1)} fusion(bf16[512,2048]{1,0:T(8,128)(2,1)} %copy-done.12, bf16[1024,2048]{1,0:T(8,128)(2,1)} %copy-done.11, bf16[2048,512]{1,0:T(8,128)(2,1)S(1)} %copy-done.6), kind=kOutput, calls=%fused_computation | convolution fusion | flops 4298637312 | bytes 12582912 | tf_op jit(solution)/shard_map/dot_general | solution.py:589
  183.4 0.0 copy-start.1
  183.4 2.2 copy-done.1
  185.6 36.6 %shard_map.131 = bf16[256,512]{1,0:T(8,128)(2,1)S(1)} custom-call(bf16[1024,2048]{1,0:T(8,128)(2,1)S(1)} %copy-done.1, bf16[256,512]{1,0:T(8,128)(2,1)S(1)} %get-tuple-element.17.refs_0_.refs_1_), custom_call_target="tpu_custom_call" | custom-call | flops 1000000000 | bytes 100000000 | tf_op jit(solution)/shard_map/pallas_call | solution.py:459
  222.2 0.7 copy.17
  (1 shorter events, 0.0 us)
Async XLA Ops:
  0.0 0.8 copy-start
  3.9 1.0 copy-start.3
  3.9 1.1 copy-start.7
  4.0 1.1 copy-start.8
  4.0 1.1 copy-start.10
  67.4 1.6 copy-start.2
  69.0 43.9 %copy-start.4 = (bf16[2048,512]{1,0:T(8,128)(2,1)S(1)}, bf16[2048,512]{1,0:T(8,128)(2,1)}, u32[]{:S(2)}) copy-start(bf16[2048,512]{1,0:T(8,128)(2,1)} %refs_3_.1) | copy-start | bytes 6291460
  69.0 43.9 %copy-start.9 = (f32[2048]{0:T(1024)S(1)}, f32[2048]{0:T(1024)}, u32[]{:S(2)}) copy-start(f32[2048]{0:T(1024)} %param.15) | copy-start | bytes 24580
  111.5 1.4 copy-start.5
  112.9 62.2 %copy-start.6 = (bf16[2048,512]{1,0:T(8,128)(2,1)S(1)}, bf16[2048,512]{1,0:T(8,128)(2,1)}, u32[]{:S(2)}) copy-start(bf16[2048,512]{1,0:T(8,128)(2,1)} %copy-done.5) | copy-start | bytes 6291460
  171.8 2.0 copy-start.11
  173.8 1.4 copy-start.12
  183.4 2.2 copy-start.1

commit v4 on v3

--- a/solution.py
+++ b/solution.py
@@ -225,14 +225,18 @@
     return jax.ShapeDtypeStruct(tuple(shape), weight.dtype)
 
 
-def gather_kernel(count, axes, *refs):
+def gather_kernel(count, axes, shared, *refs):
     held, send_z, send_x, send_c, arrived, moves, extra_sems = refs[-7:]
     own_ref, gain_ref, extra_ref = refs[:3]
     number = len(axes)
     out_ref, extra_out = refs[3 + number : 5 + number]
+    targets = list(refs[5 + number : -7])
+    if shared:
+        first = targets.pop(0)
+        half = first.shape[1] // 2
+        targets = [first.at[:, pl.ds(0, half)], first.at[:, pl.ds(half, half)]] + targets
     exchanges = [
-        Exchange(count, axis, refs[3 + k], refs[5 + number + k], moves.at[k])
-        for k, axis in enumerate(axes)
+        Exchange(count, axis, refs[3 + k], targets[k], moves.at[k]) for k, axis in enumerate(axes)
     ]
     place, row = lax.axis_index("fs"), lax.axis_index("tp")
     across, beside, corner = row ^ 2, row ^ 1, row ^ 3
@@ -328,20 +332,24 @@
         moving.wait_send()
 
 
-def gather_normed(rows, norm_gain, extra, weights, axes, number):
+def gather_normed(rows, norm_gain, extra, weights, axes, number, shared=False):
     count = lax.axis_size("fs")
     length, width = rows.shape
+    joined = [joined_shape(weight, axis, count) for weight, axis in zip(weights, axes)]
+    if shared:
+        deep, wide = joined.pop(0).shape
+        joined[0] = jax.ShapeDtypeStruct((deep, 2 * wide), rows.dtype)
     vmem = pl.BlockSpec(memory_space=pltpu.VMEM)
     dma = pltpu.SemaphoreType.DMA
     return pl.pallas_call(
-        functools.partial(gather_kernel, count, axes),
+        functools.partial(gather_kernel, count, axes, shared),
         out_shape=[
             jax.ShapeDtypeStruct((count * length, 4 * width), rows.dtype),
             jax.ShapeDtypeStruct((count, 1, length), extra.dtype),
         ]
-        + [joined_shape(weight, axis, count) for weight, axis in zip(weights, axes)],
+        + joined,
         in_specs=[vmem] * (3 + len(axes)),
-        out_specs=[vmem] * (2 + len(axes)),
+        out_specs=[vmem] * (2 + len(joined)),
         scratch_shapes=[
             pltpu.VMEM((count, 4, length, width), rows.dtype),
             dma((count,)),
@@ -552,19 +560,14 @@
         width = value.shape[axis] // count
         return lax.dynamic_slice_in_dim(value, mine * width, width, axis)
 
-    depth = gate_projection_weight.shape[0]
-    paired = [
-        weight.reshape(depth, count, -1)
-        for weight in (gate_projection_weight, recurrent_projection_weight)
-    ]
-    paired = jnp.concatenate(paired, axis=2).reshape(depth, -1)
     normed, extra, both_weight, out_weight = gather_normed(
         tokens,
         recurrent_norm_gain,
         extra_log_decay,
-        (paired, output_projection_weight),
-        (1, 0),
+        (gate_projection_weight, recurrent_projection_weight, output_projection_weight),
+        (1, 1, 0),
         1,
+        shared=True,
     )
     mixed = recurrence(
         jnp.dot(normed, both_weight, preferred_element_type=jnp.float32),

time: 224 us -> 225 us (level)
    unnamed x28 -> x31, local copies, waits for them, and re-layouts: 8.45 us -> 12 us
    reshape x2 -> x0, local copies, waits for them, and re-layouts: 2.33 us -> none  [per_device_owned(): weight.reshape(depth, count, -1)]
where the time goes in v4:
time: 225 us; the launch traced here: 224 us
  Pallas kernels  199 us (88%)
  local copies, waits for them, and re-layouts  13 us (6%)
  matrix products  10.8 us (5%)
    pallas_call x2, Pallas kernels, gather_normed(): pl.pallas_call(functools.partial(gather_kernel, count, axes, shared), out...  118 us
    pallas_call x2, Pallas kernels, scatter_added(): pl.pallas_call(functools.partial(scatter_kernel, count, axes), out_shape=...  79.3 us
    unnamed x31, local copies, waits for them, and re-layouts  12 us
    dot_general x1, matrix products, per_device_owned(): jnp.dot(squared, down_weight, preferred_element_type=jnp.float32)  8.3 us

profile of v4, /device:TPU:0, one launch (start us, length us, event | category | flops | bytes accessed | tf_op | source)
XLA Modules:
  0.0 223.8 jit_solution(2846562786163874301)
XLA Ops:
  0.0 0.0 copy-start
  0.0 0.8 fusion.1.rate_ref
  0.8 0.0 copy-done
  0.8 0.8 constant_dynamic-slice_fusion
  1.6 0.0 copy-start.3
  1.6 0.9 copy-done.3
  2.5 0.0 copy-start.6
  2.5 1.0 copy-done.6
  3.6 0.0 copy-start.7
  3.6 1.0 copy-done.7
  4.6 0.0 copy-start.8
  4.6 1.0 copy-done.8
  5.7 0.0 copy-start.9
  5.7 0.7 copy-done.9
  6.4 0.0 copy-start.11
  6.4 0.7 copy-done.11
  7.0 59.0 %shard_map.127 = (bf16[1024,2048]{1,0:T(8,128)(2,1)S(1)}, f32[4,1,256]{2,1,0:T(1,128)S(1)}, bf16[2048,256]{1,0:T(8,128)(2,1)S(1)}, bf16[128,2048]{1,0:T(8,128)(2,1)S(1)}) custom-call(bf16[256,512]{1,0:T(8,128)(2,1)S(1)} %copy-done.3, f32[1,2048]{1,0:T(1,128)S(1)} %bitcast.14, f32[1,1,256]{2,1,0:T(1,128)S(1)} %bitcast.16, bf16[512,512]{1,0:T(8,128)(2,1)S(1)} %copy-done.6, ...), custom_call_target="tpu_custom_call" | custom-call | flops 1000000000 | bytes 100000000 | tf_op jit(solution)/shard_map/pallas_call | solution.py:344
  66.0 1.3 fusion.3.gate_ref.recur_ref
  67.3 0.2 copy.14.extra_ref
  67.5 2.0 shard_map.128
  69.5 0.0 copy-start.2
  69.6 0.0 copy-start.4
  69.6 1.2 convolution_convert_fusion.1.refs_0_
  70.8 0.3 copy-done.2
  71.1 0.0 copy-done.4
  71.1 0.0 copy-start.5
  71.1 0.0 copy-start.10
  71.1 0.0 copy-start.12
  71.2 42.5 %shard_map.129 = (bf16[256,512]{1,0:T(8,128)(2,1)S(1)}, bf16[2048,512]{1,0:T(8,128)(2,1)S(1)}) custom-call(bf16[1024,2048]{1,0:T(8,128)(2,1)S(1)} %convolution_convert_fusion.1.refs_0_, bf16[256,512]{1,0:T(8,128)(2,1)S(1)} %copy-done.4, bf16[512,2048]{1,0:T(8,128)(2,1)S(1)} %copy-done.2), custom_call_target="tpu_custom_call" | custom-call | flops 1000000000 | bytes 100000000 | tf_op jit(solution)/shard_map/pallas_call | solution.py:467
  113.7 0.0 copy-done.5
  113.7 0.0 copy-done.10
  113.7 0.0 copy-done.12
  113.7 58.8 %shard_map.130 = (bf16[1024,2048]{1,0:T(8,128)(2,1)S(1)}, f32[4,1,256]{2,1,0:T(1,128)}, bf16[512,2048]{1,0:T(8,128)(2,1)S(1)}) custom-call(bf16[256,512]{1,0:T(8,128)(2,1)S(1)} %get-tuple-element.17.refs_0_.refs_1_, f32[1,2048]{1,0:T(1,128)S(1)} %bitcast.15, f32[1,1,256]{2,1,0:T(1,128)S(1)} %bitcast.17, bf16[2048,512]{1,0:T(8,128)(2,1)S(1)} %copy-done.5), custom_call_target="tpu_custom_call" | custom-call | flops 1000000000 | bytes 100000000 | tf_op jit(solution)/shard_map/pallas_call | solution.py:344
  172.5 0.0 copy-start.13
  172.5 1.9 copy-done.13
  174.5 0.0 copy-start.14
  174.5 1.4 copy-done.14
  175.9 8.3 %convolution_convert_fusion.refs_0_ = bf16[1024,2048]{1,0:T(8,128)(2,1)} fusion(bf16[512,2048]{1,0:T(8,128)(2,1)} %copy-done.14, bf16[1024,2048]{1,0:T(8,128)(2,1)} %copy-done.13, bf16[2048,512]{1,0:T(8,128)(2,1)S(1)} %get-tuple-element.19), kind=kOutput, calls=%fused_computation | convolution fusion | flops 4298637312 | bytes 12582912 | tf_op jit(solution)/shard_map/dot_general | solution.py:592
  184.2 0.0 copy-start.1
  184.2 2.2 copy-done.1
  186.4 36.7 %shard_map.131 = bf16[256,512]{1,0:T(8,128)(2,1)S(1)} custom-call(bf16[1024,2048]{1,0:T(8,128)(2,1)S(1)} %copy-done.1, bf16[256,512]{1,0:T(8,128)(2,1)S(1)} %get-tuple-element.17.refs_0_.refs_1_), custom_call_target="tpu_custom_call" | custom-call | flops 1000000000 | bytes 100000000 | tf_op jit(solution)/shard_map/pallas_call | solution.py:467
  223.1 0.7 copy.16
  (1 shorter events, 0.0 us)
Async XLA Ops:
  0.0 0.8 copy-start
  1.6 0.9 copy-start.3
  2.5 1.0 copy-start.6
  3.6 1.0 copy-start.7
  4.6 1.0 copy-start.8
  5.7 0.7 copy-start.9
  6.4 0.7 copy-start.11
  69.5 1.6 copy-start.2
  69.6 1.6 copy-start.4
  71.1 42.6 %copy-start.5 = (bf16[2048,512]{1,0:T(8,128)(2,1)S(1)}, bf16[2048,512]{1,0:T(8,128)(2,1)}, u32[]{:S(2)}) copy-start(bf16[2048,512]{1,0:T(8,128)(2,1)} %refs_3_.3) | copy-start | bytes 6291460
  71.1 42.6 %copy-start.10 = (f32[2048]{0:T(1024)S(1)}, f32[2048]{0:T(1024)}, u32[]{:S(2)}) copy-start(f32[2048]{0:T(1024)} %param.15) | copy-start | bytes 24580
  71.1 42.6 %copy-start.12 = (f32[256]{0:T(256)S(1)}, f32[256]{0:T(256)}, u32[]{:S(2)}) copy-start(f32[256]{0:T(256)} %param.22) | copy-start | bytes 3076
  172.5 2.0 copy-start.13
  174.5 1.4 copy-start.14
  184.2 2.2 copy-start.1
